TPU v7x, 512 devices: a whole 4x4x16 slice. The times are simulated.
512 devices in a mesh: rep: 2 (over z_hi), fs: 32 (over z_lo, y), tp: 8 (over x, core).
Axes of the slice: x: 4, y: 4, z: 16 (z_hi: 2, z_lo: 8; z = z_hi * 8 + z_lo), core: 2. Of those that a mesh axis runs over, the one named last changes fastest.
Arguments:
- stream: bfloat16 [16384, 2048], P(('rep', 'fs'), 'tp'), may hold values from -6 to 6
- norm_gains: float32 [6, 2048], replicated, may hold values from 0.1 to 1.9
- w_gate: bfloat16 [2048, 5632], P('fs', 'tp'), may hold values from -0.125 to 0.125
- w_up: bfloat16 [2048, 5632], P('fs', 'tp'), may hold values from -0.125 to 0.125
- w_down: bfloat16 [5632, 2048], P('tp', 'fs'), may hold values from -0.15625 to 0.15625
- w_inner: bfloat16 [2048, 1024], P('fs', 'tp'), may hold values from -0.125 to 0.125
- w_bgate: bfloat16 [2048, 1024], P('fs', 'tp'), may hold values from -0.125 to 0.125
- w_cgate: bfloat16 [2048, 1024], P('fs', 'tp'), may hold values from -0.125 to 0.125
- conv_taps: float32 [3, 1024], P(None, 'tp'), may hold values from -3.5 to 3.5
- w_out: bfloat16 [1024, 2048], P('tp', 'fs'), may hold values from -0.375 to 0.375
Outputs:
- mixed: bfloat16 [16384, 2048], P(('rep', 'fs'), 'tp')
All inputs are finite; a program needn't handle non-finite values.
Results may differ from a plain program's by a relative error of at most 0.02.
Values may be sent and summed in bfloat16 or wider, within the bound.
A program may use at most 64 MiB of HBM per device.

v0:
```python
import jax
import jax.numpy as jnp
from jax import lax
from jax.sharding import PartitionSpec as P

TAPS = 3


EPSILON = 1e-06


def laid_out(parts, dim):
    shape = list(parts.shape[1:])
    shape[dim] *= parts.shape[0]
    return jnp.moveaxis(parts, 0, dim).reshape(shape)


def from_everyone(x, axis):
    copies = jnp.broadcast_to(x, (lax.axis_size(axis), *x.shape))
    return lax.all_to_all(copies, axis, split_axis=0, concat_axis=0, tiled=True)


def collect(x, axis, dim):
    return laid_out(from_everyone(x, axis), dim)


def cut_along(x, dim, count):
    shape = x.shape
    parts = x.reshape(*shape[:dim], count, shape[dim] // count, *shape[dim + 1 :])
    return jnp.moveaxis(parts, dim, 0)


def sent_and_summed(x, axis, dim):
    parts = cut_along(x, dim, lax.axis_size(axis))
    arrived = lax.all_to_all(parts, axis, split_axis=0, concat_axis=0, tiled=True)
    return arrived.astype(jnp.float32).sum(axis=0)


def taken_together(x, axis):
    everything = from_everyone(x, axis)
    return jnp.sum(everything, axis=0)


def rows_first(arrays, axis, dims):
    turned = [jnp.moveaxis(a, dim, 0) for a, dim in zip(arrays, dims)]
    both = jnp.concatenate([t.reshape(len(t), -1) for t in turned], axis=1)
    whole, at, done = (lax.all_gather(both, axis, axis=0, tiled=True), 0, [])
    for t, dim in zip(turned, dims):
        slab = whole[:, at : at + t[0].size].reshape(-1, *t.shape[1:])
        done.append(jnp.moveaxis(slab, 0, dim))
        at += t[0].size
    return tuple(done)


def from_behind(x, axis, by):
    count = lax.axis_size(axis)
    pairs = [(i, i + by) for i in range(count) if 0 <= i + by < count]
    return lax.ppermute(x, axis, pairs)


def shards(stream, norm_gains, w_gate, w_up, w_down, w_inner, w_bgate, w_cgate, conv_taps, w_out):
    tp_index = lax.axis_index("tp")
    local_width = stream.shape[1]
    model_width = local_width * lax.axis_size("tp")

    def own_gain(row):
        return lax.dynamic_slice_in_dim(norm_gains[row], tp_index * local_width, local_width, 0)

    def gathered_norm(current, row):
        gathered = collect(current, "tp", 1)
        values = gathered.astype(jnp.float32)
        scaled = values * lax.rsqrt(jnp.mean(values * values, axis=1, keepdims=True) + EPSILON)
        return (scaled * norm_gains[row]).astype(jnp.bfloat16)

    def settle(current, partials, row, weight):
        branch_sum = sent_and_summed(partials.astype(jnp.bfloat16), "tp", 1)
        squares = taken_together(jnp.sum(branch_sum * branch_sum, axis=1), "tp")
        scaled = branch_sum * lax.rsqrt(squares / model_width + EPSILON)[:, None]
        return (current.astype(jnp.float32) + weight * (scaled * own_gain(row))).astype(
            jnp.bfloat16
        )

    gate_whole, up_whole, down_whole = rows_first((w_gate, w_up, w_down), "fs", (0, 0, 1))

    def feed_forward(current, row_in, row_out):
        normed = gathered_norm(current, row_in)
        gate_vals = jnp.dot(normed, gate_whole, preferred_element_type=jnp.float32)
        upward = jnp.dot(normed, up_whole, preferred_element_type=jnp.float32)
        hidden = (jax.nn.silu(gate_vals) * upward).astype(jnp.bfloat16)
        partials = jnp.dot(hidden, down_whole, preferred_element_type=jnp.float32)
        return settle(current, partials, row_out, 0.5)

    first = feed_forward(stream, 0, 1)
    normed_mix = gathered_norm(first, 2)
    local_rows = normed_mix.shape[0]

    def fold_rows(block_rows):
        return jnp.dot(normed_mix, block_rows, preferred_element_type=jnp.float32)

    inner = fold_rows(collect(w_inner, "fs", 0))
    bgate = fold_rows(collect(w_bgate, "fs", 0))
    cgate = fold_rows(collect(w_cgate, "fs", 0))
    conv_input = cgate * inner
    earlier = from_behind(conv_input[local_rows - (TAPS - 1) :], "fs", 1)
    padded = jnp.concatenate([earlier, conv_input], axis=0)
    conv = conv_taps[0] * padded[0:local_rows]
    for tap in range(1, TAPS):
        conv = conv + conv_taps[tap] * padded[tap : tap + local_rows]
    gated = (bgate * conv).astype(jnp.bfloat16)
    mix_partials = jnp.dot(gated, collect(w_out, "fs", 1), preferred_element_type=jnp.float32)
    second = settle(first, mix_partials, 3, 1.0)
    return feed_forward(second, 4, 5)


def solution(mesh):
    return jax.shard_map(
        shards,
        mesh=mesh,
        in_specs=(
            P(("rep", "fs"), "tp"),
            P(),
            P("fs", "tp"),
            P("fs", "tp"),
            P("tp", "fs"),
            P("fs", "tp"),
            P("fs", "tp"),
            P("fs", "tp"),
            P(None, "tp"),
            P("tp", "fs"),
        ),
        out_specs=P(("rep", "fs"), "tp"),
        check_vma=False,
    )
```

profile of v0, /device:TPU:1, one launch (start us, length us, event | category | flops | bytes accessed | tf_op | source)
XLA Modules:
  0.0 521.1 jit_solution(112186578533772279)
XLA Ops:
  6.5 1.8 concatenate.6
  8.4 0.0 all-gather.2.cloned.1.call-update
  8.4 1.0 copy.27
  9.4 0.1 broadcast_in_dim.39
  9.5 24.3 %all_to_all.68 = bf16[8,256,256]{1,2,0:T(8,128)(2,1)S(1)} all-to-all(bf16[8,256,256]{1,2,0:T(8,128)(2,1)S(1)} %broadcast_in_dim.39), channel_id=1, replica_groups=mesh['rep'=2,'fs'=32,'tp'=8] {'tp'}, dimensions={0} | all-to-all | bytes 2097152 | tf_op jit(solution)/shard_map/all_to_all | solution.py:20
  33.8 1.0 broadcast_in_dim.43
  34.8 11.8 %all-to-all-start.5 = ((bf16[32,64,128]{2,1,0:T(8,128)(2,1)}), bf16[32,64,128]{2,1,0:T(8,128)(2,1)S(1)}, u32[]{:S(2)}, u32[]{:S(2)}) async-start(bf16[32,64,128]{2,1,0:T(8,128)(2,1)} %broadcast_in_dim.43), calls=%async_computation.5 | async-start | bytes 1048576 | tf_op jit(solution)/shard_map/all_to_all | solution.py:20
  46.7 0.6 fusion.67
  47.3 0.3 multiply_reduce_fusion.1
  47.6 0.3 fusion.24
  48.0 186.2 %all-gather.2.cloned.1.call-done = bf16[2048,2112]{1,0:T(8,128)(2,1)} async-done(((bf16[64,2112]{1,0:T(8,128)(2,1)}), bf16[2048,2112]{1,0:T(8,128)(2,1)}) %all-gather.2.cloned.1.call-update) | async-done | bytes 8650768 | tf_op jit(solution)/shard_map/all_gather | solution.py:47
  234.2 3.2 fusion.10
  237.4 7.4 %fusion.12 = bf16[256,2048]{1,0:T(8,128)(2,1)S(1)} fusion(bf16[2048,2112]{1,0:T(8,128)(2,1)} %all-gather.2.cloned.1.call-done, bf16[256,2048]{0,1:T(8,128)(2,1)S(1)} %fusion.24, f32[256,704]{0,1:T(8,128)S(1)} %fusion.10), kind=kOutput, calls=%fused_computation.15 | convolution fusion | flops 1478000640 | bytes 9109504 | tf_op jit(solution)/shard_map/dot_general | solution.py:90
  244.8 0.1 copy.47
  244.9 0.9 copy-done
  245.8 41.3 %all_to_all.69 = bf16[8,256,256]{2,1,0:T(8,128)(2,1)S(1)} all-to-all(bf16[8,256,256]{2,1,0:T(8,128)(2,1)S(1)} %bitcast.73), channel_id=1, replica_groups=mesh['rep'=2,'fs'=32,'tp'=8] {'tp'}, dimensions={0} | all-to-all | bytes 2097152 | tf_op jit(solution)/shard_map/all_to_all | solution.py:35
  287.1 0.9 broadcast_in_dim.44
  288.0 8.5 %all-to-all-start.6 = ((bf16[32,64,128]{2,1,0:T(8,128)(2,1)}), bf16[32,64,128]{2,1,0:T(8,128)(2,1)S(1)}, u32[]{:S(2)}, u32[]{:S(2)}) async-start(bf16[32,64,128]{2,1,0:T(8,128)(2,1)} %broadcast_in_dim.44), calls=%async_computation.6 | async-start | bytes 1048576 | tf_op jit(solution)/shard_map/all_to_all | solution.py:20
  296.5 0.1 convert_reduce_fusion.2
  296.7 0.1 multiply_reduce_fusion.4
  296.8 26.5 %all-to-all-done.6 = bf16[32,64,128]{2,1,0:T(8,128)(2,1)S(1)} async-done(((bf16[32,64,128]{2,1,0:T(8,128)(2,1)}), bf16[32,64,128]{2,1,0:T(8,128)(2,1)S(1)}, u32[]{:S(2)}, u32[]{:S(2)}) %all-to-all-start.6) | async-done | bytes 524320 | tf_op jit(solution)/shard_map/all_to_all | solution.py:20
  323.3 10.8 %all_to_all.70 = f32[8,1,256]{2,1,0:T(1,128)S(1)} all-to-all(f32[8,1,256]{2,1,0:T(1,128)S(1)} %broadcast_in_dim.40), channel_id=1, replica_groups=mesh['rep'=2,'fs'=32,'tp'=8] {'tp'}, dimensions={0} | all-to-all | bytes 16384 | tf_op jit(solution)/shard_map/all_to_all | solution.py:20
  334.1 0.9 broadcast_in_dim.45
  335.0 5.8 %all-to-all-start.7 = ((bf16[32,128,64]{1,2,0:T(8,128)(2,1)}), bf16[32,128,64]{1,2,0:T(8,128)(2,1)S(1)}, u32[]{:S(2)}, u32[]{:S(2)}) async-start(bf16[32,128,64]{1,2,0:T(8,128)(2,1)} %broadcast_in_dim.45), calls=%async_computation.7 | async-start | bytes 1048576 | tf_op jit(solution)/shard_map/all_to_all | solution.py:20
  340.8 0.6 constant_dynamic-slice_fusion.2
  341.5 0.1 add_convert_fusion.2
  341.6 0.1 copy.30
  341.7 25.8 %all-to-all-done.7 = bf16[32,128,64]{1,2,0:T(8,128)(2,1)S(1)} async-done(((bf16[32,128,64]{1,2,0:T(8,128)(2,1)}), bf16[32,128,64]{1,2,0:T(8,128)(2,1)S(1)}, u32[]{:S(2)}, u32[]{:S(2)}) %all-to-all-start.7) | async-done | bytes 524320 | tf_op jit(solution)/shard_map/all_to_all | solution.py:20
  367.6 0.1 broadcast_in_dim.41
  367.6 21.2 %all_to_all.71 = bf16[8,256,256]{1,2,0:T(8,128)(2,1)S(1)} all-to-all(bf16[8,256,256]{1,2,0:T(8,128)(2,1)S(1)} %broadcast_in_dim.41), channel_id=1, replica_groups=mesh['rep'=2,'fs'=32,'tp'=8] {'tp'}, dimensions={0} | all-to-all | bytes 2097152 | tf_op jit(solution)/shard_map/all_to_all | solution.py:20
  388.8 0.9 broadcast_in_dim.42
  389.7 5.9 %all-to-all-start.4 = ((bf16[32,64,128]{2,1,0:T(8,128)(2,1)}), bf16[32,64,128]{2,1,0:T(8,128)(2,1)}, u32[]{:S(2)}, u32[]{:S(2)}) async-start(bf16[32,64,128]{2,1,0:T(8,128)(2,1)} %broadcast_in_dim.42), calls=%async_computation.4 | async-start | bytes 1048576 | tf_op jit(solution)/shard_map/all_to_all | solution.py:20
  395.7 0.3 fusion.18
  396.0 0.3 fusion.20
  396.4 1.5 fusion.70
  397.9 0.5 convolution_multiply_fusion
  398.4 3.1 collective-permute-start
  401.5 20.9 %all-to-all-done.4 = bf16[32,64,128]{2,1,0:T(8,128)(2,1)} async-done(((bf16[32,64,128]{2,1,0:T(8,128)(2,1)}), bf16[32,64,128]{2,1,0:T(8,128)(2,1)}, u32[]{:S(2)}, u32[]{:S(2)}) %all-to-all-start.4) | async-done | bytes 524320 | tf_op jit(solution)/shard_map/all_to_all | solution.py:20
  422.4 1.9 convolution_convert_fusion
  424.3 0.1 copy.46
  424.4 21.4 %all_to_all.72 = bf16[8,256,256]{2,1,0:T(8,128)(2,1)S(1)} all-to-all(bf16[8,256,256]{2,1,0:T(8,128)(2,1)S(1)} %bitcast.74), channel_id=1, replica_groups=mesh['rep'=2,'fs'=32,'tp'=8] {'tp'}, dimensions={0} | all-to-all | bytes 2097152 | tf_op jit(solution)/shard_map/all_to_all | solution.py:35
  445.7 0.1 convert_reduce_fusion.1
  445.9 0.1 multiply_reduce_fusion.3
  446.0 0.6 broadcast_in_dim.46
  446.6 4.3 all-to-all-start.9
  450.9 0.6 constant_dynamic-slice_fusion.1
  451.5 4.0 all-to-all-done.9
  455.5 0.1 add_convert_fusion.1
  455.6 0.1 copy.33
  455.8 0.1 broadcast_in_dim.47
  455.8 18.1 %all_to_all.73 = bf16[8,256,256]{1,2,0:T(8,128)(2,1)S(1)} all-to-all(bf16[8,256,256]{1,2,0:T(8,128)(2,1)S(1)} %broadcast_in_dim.47), channel_id=1, replica_groups=mesh['rep'=2,'fs'=32,'tp'=8] {'tp'}, dimensions={0} | all-to-all | bytes 2097152 | tf_op jit(solution)/shard_map/all_to_all | solution.py:20
  473.9 0.3 multiply_reduce_fusion
  474.2 0.3 fusion.22
  474.5 3.2 fusion.8
  477.7 7.4 %fusion.15 = bf16[256,2048]{1,0:T(8,128)(2,1)S(1)} fusion(bf16[2048,2112]{1,0:T(8,128)(2,1)} %all-gather.2.cloned.1.call-done, bf16[256,2048]{0,1:T(8,128)(2,1)S(1)} %fusion.22, f32[256,704]{0,1:T(8,128)S(1)} %fusion.8), kind=kOutput, calls=%fused_computation.16 | convolution fusion | flops 1478000640 | bytes 9109504 | tf_op jit(solution)/shard_map/dot_general | solution.py:90
  485.2 0.1 copy.45
  485.2 18.4 %all_to_all.74 = bf16[8,256,256]{2,1,0:T(8,128)(2,1)S(1)} all-to-all(bf16[8,256,256]{2,1,0:T(8,128)(2,1)S(1)} %bitcast.75), channel_id=1, replica_groups=mesh['rep'=2,'fs'=32,'tp'=8] {'tp'}, dimensions={0} | all-to-all | bytes 2097152 | tf_op jit(solution)/shard_map/all_to_all | solution.py:35
  503.6 0.1 convert_reduce_fusion
  503.8 0.1 multiply_reduce_fusion.2
  503.9 0.6 broadcast_in_dim.48
  504.5 4.3 all-to-all-start.12
  508.8 0.7 constant_dynamic-slice_fusion
  509.4 4.0 all-to-all-done.12
  513.4 0.8 add_convert_fusion
  (31 shorter events, 0.2 us)
Async XLA Ops:
  6.5 227.7 %all-gather.2.cloned.1.call-start = ((), (), s32[]{:S(2)}) async-start(), calls=%async_computation.13 | async-start | bytes 9191424 | tf_op jit(solution)/shard_map/all_gather | solution.py:47
  6.5 27.3 %copy-start.3 = (bf16[64,128]{1,0:T(8,128)(2,1)S(1)}, bf16[64,128]{1,0:T(8,128)(2,1)}, u32[]{:S(2)}) copy-start(bf16[64,128]{1,0:T(8,128)(2,1)} %param.17) | copy-start | bytes 49156
  9.5 37.2 %copy-start.2 = (f32[6,2048]{1,0:T(8,128)S(1)}, f32[6,2048]{1,0:T(8,128)}, u32[]{:S(2)}) copy-start(f32[6,2048]{1,0:T(8,128)} %param.11) | copy-start | bytes 147460
  34.8 210.1 %all-to-all-start.5 = ((bf16[32,64,128]{2,1,0:T(8,128)(2,1)}), bf16[32,64,128]{2,1,0:T(8,128)(2,1)S(1)}, u32[]{:S(2)}, u32[]{:S(2)}) async-start(bf16[32,64,128]{2,1,0:T(8,128)(2,1)} %broadcast_in_dim.43), calls=%async_computation.5 | async-start | bytes 1048576 | tf_op jit(solution)/shard_map/all_to_all | solution.py:20
  244.9 42.2 %copy-start.4 = (bf16[64,128]{1,0:T(8,128)(2,1)S(1)}, bf16[64,128]{1,0:T(8,128)(2,1)}, u32[]{:S(2)}) copy-start(bf16[64,128]{1,0:T(8,128)(2,1)} %param.15) | copy-start | bytes 49156
  244.9 0.9 copy-start
  287.1 47.0 %copy-start.5 = (bf16[128,64]{0,1:T(8,128)(2,1)S(1)}, bf16[128,64]{0,1:T(8,128)(2,1)}, u32[]{:S(2)}) copy-start(bf16[128,64]{0,1:T(8,128)(2,1)} %param.19) | copy-start | bytes 49156
  288.0 53.5 %copy-start.1 = (bf16[256,256]{1,0:T(8,128)(2,1)S(1)}, bf16[256,256]{1,0:T(8,128)(2,1)}, u32[]{:S(2)}) copy-start(bf16[256,256]{1,0:T(8,128)(2,1)} %param.10) | copy-start | bytes 393220
  288.0 35.3 %all-to-all-start.6 = ((bf16[32,64,128]{2,1,0:T(8,128)(2,1)}), bf16[32,64,128]{2,1,0:T(8,128)(2,1)S(1)}, u32[]{:S(2)}, u32[]{:S(2)}) async-start(bf16[32,64,128]{2,1,0:T(8,128)(2,1)} %broadcast_in_dim.44), calls=%async_computation.6 | async-start | bytes 1048576 | tf_op jit(solution)/shard_map/all_to_all | solution.py:20
  335.0 32.6 %all-to-all-start.7 = ((bf16[32,128,64]{1,2,0:T(8,128)(2,1)}), bf16[32,128,64]{1,2,0:T(8,128)(2,1)S(1)}, u32[]{:S(2)}, u32[]{:S(2)}) async-start(bf16[32,128,64]{1,2,0:T(8,128)(2,1)} %broadcast_in_dim.45), calls=%async_computation.7 | async-start | bytes 1048576 | tf_op jit(solution)/shard_map/all_to_all | solution.py:20
  340.8 48.0 %copy-start.6 = (bf16[64,128]{1,0:T(8,128)(2,1)S(1)}, bf16[64,128]{1,0:T(8,128)(2,1)}, u32[]{:S(2)}) copy-start(bf16[64,128]{1,0:T(8,128)(2,1)} %param.16) | copy-start | bytes 49156
  389.7 32.7 %all-to-all-start.4 = ((bf16[32,64,128]{2,1,0:T(8,128)(2,1)}), bf16[32,64,128]{2,1,0:T(8,128)(2,1)}, u32[]{:S(2)}, u32[]{:S(2)}) async-start(bf16[32,64,128]{2,1,0:T(8,128)(2,1)} %broadcast_in_dim.42), calls=%async_computation.4 | async-start | bytes 1048576 | tf_op jit(solution)/shard_map/all_to_all | solution.py:20
  396.4 5.1 copy-start.7
  398.4 24.0 %collective-permute-start = (f32[2,128]{1,0:T(2,128)S(1)}, f32[2,128]{1,0:T(2,128)S(1)}, u32[]{:S(2)}, u32[]{:S(2)}) collective-permute-start(f32[2,128]{1,0:T(2,128)S(1)} %slice.63), channel_id=1, source_target_pairs={{0,8},{8,16},{16,24},{24,32},{32,40},{40,48},{48,56},{56,64},{64,7... | collective-permute-start | bytes 3080 | tf_op jit(solution)/shard_map/ppermute | solution.py:58
  446.6 8.9 %all-to-all-start.9 = ((f32[8,1,256]{2,1,0:T(1,128)}), f32[8,1,256]{2,1,0:T(1,128)S(1)}, u32[]{:S(2)}, u32[]{:S(2)}) async-start(f32[8,1,256]{2,1,0:T(1,128)} %broadcast_in_dim.46), calls=%async_computation.9 | async-start | bytes 16384 | tf_op jit(solution)/shard_map/all_to_all | solution.py:20
  504.5 8.9 %all-to-all-start.12 = ((f32[8,1,256]{2,1,0:T(1,128)}), f32[8,1,256]{2,1,0:T(1,128)S(1)}, u32[]{:S(2)}, u32[]{:S(2)}) async-start(f32[8,1,256]{2,1,0:T(1,128)} %broadcast_in_dim.48), calls=%async_computation.12 | async-start | bytes 16384 | tf_op jit(solution)/shard_map/all_to_all | solution.py:20
Sparse Core Ops, SparseCore 0:
  9.4 224.7 all-gather.1
where the time goes:
time: 522 us; the launch traced here: 521 us
  waiting for transfers between devices  267 us (51%)
  blocking collectives  155 us (30%)
  starting transfers between devices  43.7 us (8%)
  matrix products  25 us (5%)
  between operations  13.7 us (3%)
  local copies, waits for them, and re-layouts  11.8 us (2%)
    all_gather x1, waiting for transfers between devices, rows_first(): whole, at, done = (lax.all_gather(both, axis, axis=0, tiled=True), 0, [])  186 us
    all_to_all x6, waiting for transfers between devices, from_everyone(): return lax.all_to_all(copies, axis, split_axis=0, concat_axis=0, tiled=True)  81.2 us
    all_to_all x3, blocking collectives, sent_and_summed(): lax.all_to_all(parts, axis, split_axis=0, concat_axis=0, tiled=True)  81.1 us
    all_to_all x4, blocking collectives, from_everyone(): return lax.all_to_all(copies, axis, split_axis=0, concat_axis=0, tiled=True)  74.4 us
    all_to_all x6, starting transfers between devices, from_everyone(): return lax.all_to_all(copies, axis, split_axis=0, concat_axis=0, tiled=True)  40.6 us
    dot_general x2, matrix products, feed_forward(): partials = jnp.dot(hidden, down_whole, preferred_element_type=jnp.float32)  14.8 us
  transfers between devices with their start and end apart: 8, of which 6 were waited for; matrix products, arithmetic and copies ran while one was open for 4% of the time, Pallas kernels for 0%

commit v1 on v0

--- a/solution.py
+++ b/solution.py
@@ -1,12 +1,167 @@
 import jax
 import jax.numpy as jnp
 from jax import lax
+from jax.experimental import pallas as pl
+from jax.experimental.pallas import tpu as pltpu
 from jax.sharding import PartitionSpec as P
 
 TAPS = 3
-
-
 EPSILON = 1e-06
+Z_LO, Z_ALL, Y = 8, 16, 4
+ROWS = 64
+PARTS = (
+    ((0, 640, "y"), (640, 768, "z")),
+    ((0, 256, "y"), (256, 512, "z")),
+    ((0, 128, "y"), (128, 384, "z")),
+)
+WIDTHS = (1408, 768, 512)
+RATE = 46.6e3
+HOP = 2.0
+AHEAD = 4.0
+
+
+class Copy:
+    def __init__(self, number, part, link, dz, dy, row, rows, after):
+        self.number, self.part, self.link = number, part, link
+        self.dz, self.dy, self.row, self.rows = dz, dy, row, rows
+        self.after, self.tail = after, 0.0
+        stream, index = part
+        self.time = rows * PARTS[stream][index][1] * 2 / RATE
+        self.start = None
+
+
+def all_copies():
+    copies = []
+
+    def add(part, link, dz, dy, after, row=0, rows=ROWS):
+        copies.append(Copy(len(copies), part, link, dz, dy, row, rows, list(after)))
+        return copies[-1]
+
+    half = ROWS // 2
+    for stream, parts in enumerate(PARTS):
+        for index, (_, _, first) in enumerate(parts):
+            part = (stream, index)
+
+            def along_z(dy, own):
+                came = {0: own}
+                for sign, link, row in ((-1, "z+", 0), (1, "z-", half)):
+                    previous = own
+                    for step in range(3):
+                        previous = [add(part, link, sign * step, dy, previous)]
+                        came[sign * (step + 1)] = previous
+                    last = add(part, link, sign * 3, dy, previous, row, half)
+                    came.setdefault(4, []).append(last)
+                return came
+
+            def along_y(dz, own):
+                up = add(part, "y+", dz, 0, own)
+                down = add(part, "y-", dz, 0, own)
+                far = [
+                    add(part, "y+", dz, -1, [up], 0, half),
+                    add(part, "y-", dz, 1, [down], half, half),
+                ]
+                return {0: own, -1: [up], 1: [down], 2: far}
+
+            if first == "y":
+                for dy, got in along_y(0, []).items():
+                    along_z(dy, got)
+            else:
+                for dz, got in along_z(0, []).items():
+                    along_y(dz, got)
+    for copy in reversed(copies):
+        for before in copy.after:
+            before.tail = max(before.tail, copy.tail + copy.time + HOP)
+    return copies
+
+
+def planned():
+    copies = all_copies()
+    free = dict.fromkeys(("y+", "y-", "z+", "z-"), 0.0)
+    waiting, flying, here, order, now = list(copies), [], set(), [], 0.0
+    while waiting or flying:
+        ready = [c for c in waiting if all(b.number in here for b in c.after)]
+        ready.sort(key=lambda c: (c.part[0], -c.tail, c.number))
+        for copy in ready:
+            if free[copy.link] < now + AHEAD:
+                free[copy.link] = max(free[copy.link], now) + copy.time
+                flying.append((free[copy.link] + HOP, copy.number, copy))
+                waiting.remove(copy)
+                order.append(("start", copy, now))
+        flying.sort(key=lambda f: f[:2])
+        now, _, copy = flying.pop(0)
+        here.add(copy.number)
+        order.append(("wait", copy, now))
+    return order, copies
+
+
+def gather_kernel(order, copies, own0, own1, own2, full0, full1, full2, send_sem, recv_sem):
+    own, full = (own0, own1, own2), (full0, full1, full2)
+    rep, fs, tp = lax.axis_index("rep"), lax.axis_index("fs"), lax.axis_index("tp")
+    z_lo, y = fs // Y, lax.rem(fs, Y)
+    z = rep * Z_LO + z_lo
+
+    def at(z_to, y_to):
+        return (z_to // Z_LO, lax.rem(z_to, Z_LO) * Y + y_to, tp)
+
+    place = {
+        "y+": at(z, lax.rem(y + 1, Y)),
+        "y-": at(z, lax.rem(y + Y - 1, Y)),
+        "z+": at(lax.rem(z + 1, Z_ALL), y),
+        "z-": at(lax.rem(z + Z_ALL - 1, Z_ALL), y),
+    }
+    barrier = pltpu.get_barrier_semaphore()
+    for device in place.values():
+        pl.semaphore_signal(barrier, inc=1, device_id=device, device_id_type=pl.DeviceIdType.MESH)
+    pl.semaphore_wait(barrier, len(place))
+
+    def remote(copy):
+        stream, index = copy.part
+        column, width, _ = PARTS[stream][index]
+        columns = pl.ds(column, width)
+        block = lax.rem(z_lo + copy.dz + Z_LO, Z_LO) * Y + lax.rem(y + copy.dy + Y, Y)
+        rows = pl.ds(pl.multiple_of(block * ROWS, ROWS) + copy.row, copy.rows)
+        target = full[stream].at[rows, columns]
+        source = target
+        if copy.dz == 0 and copy.dy == 0:
+            source = own[stream].at[pl.ds(copy.row, copy.rows), columns]
+        return pltpu.make_async_remote_copy(
+            src_ref=source,
+            dst_ref=target,
+            send_sem=send_sem.at[copy.number],
+            recv_sem=recv_sem.at[copy.number],
+            device_id=place[copy.link],
+            device_id_type=pl.DeviceIdType.MESH,
+        )
+
+    mine = pl.ds(pl.multiple_of(fs * ROWS, ROWS), ROWS)
+    for stream in range(3):
+        full[stream][mine, :] = own[stream][...]
+    for kind, copy, _ in order:
+        if kind == "start":
+            remote(copy).start()
+        else:
+            remote(copy).wait_recv()
+    for copy in copies:
+        remote(copy).wait_send()
+
+
+def gathered_weights(pieces):
+    order, copies = planned()
+
+    def kernel(*refs):
+        gather_kernel(order, copies, *refs)
+
+    return pl.pallas_call(
+        kernel,
+        out_shape=[jax.ShapeDtypeStruct((ROWS * Z_LO * Y, w), jnp.bfloat16) for w in WIDTHS],
+        in_specs=[pl.BlockSpec(memory_space=pltpu.VMEM)] * 3,
+        out_specs=[pl.BlockSpec(memory_space=pltpu.VMEM)] * 3,
+        scratch_shapes=[
+            pltpu.SemaphoreType.DMA((len(copies),)),
+            pltpu.SemaphoreType.DMA((len(copies),)),
+        ],
+        compiler_params=pltpu.CompilerParams(collective_id=0, has_side_effects=True),
+    )(*pieces)
 
 
 def laid_out(parts, dim):
@@ -41,27 +196,25 @@
     return jnp.sum(everything, axis=0)
 
 
-def rows_first(arrays, axis, dims):
-    turned = [jnp.moveaxis(a, dim, 0) for a, dim in zip(arrays, dims)]
-    both = jnp.concatenate([t.reshape(len(t), -1) for t in turned], axis=1)
-    whole, at, done = (lax.all_gather(both, axis, axis=0, tiled=True), 0, [])
-    for t, dim in zip(turned, dims):
-        slab = whole[:, at : at + t[0].size].reshape(-1, *t.shape[1:])
-        done.append(jnp.moveaxis(slab, 0, dim))
-        at += t[0].size
-    return tuple(done)
-
-
 def from_behind(x, axis, by):
     count = lax.axis_size(axis)
     pairs = [(i, i + by) for i in range(count) if 0 <= i + by < count]
     return lax.ppermute(x, axis, pairs)
 
 
+def packed(w_gate, w_up, w_down, w_inner, w_bgate, w_cgate, w_out):
+    first = jnp.concatenate([w_gate, w_up], axis=1)
+    second = jnp.pad(w_down.T, ((0, 0), (0, 64)))
+    third = jnp.concatenate([w_inner, w_bgate, w_cgate, w_out.T], axis=1)
+    return first, second, third
+
+
 def shards(stream, norm_gains, w_gate, w_up, w_down, w_inner, w_bgate, w_cgate, conv_taps, w_out):
     tp_index = lax.axis_index("tp")
     local_width = stream.shape[1]
     model_width = local_width * lax.axis_size("tp")
+    units = w_gate.shape[1]
+    channels = w_inner.shape[1]
 
     def own_gain(row):
         return lax.dynamic_slice_in_dim(norm_gains[row], tp_index * local_width, local_width, 0)
@@ -80,26 +233,27 @@
             jnp.bfloat16
         )
 
-    gate_whole, up_whole, down_whole = rows_first((w_gate, w_up, w_down), "fs", (0, 0, 1))
+    both_whole, down_whole, mix_whole = gathered_weights(
+        packed(w_gate, w_up, w_down, w_inner, w_bgate, w_cgate, w_out)
+    )
+
+    def onto(x, turned):
+        return lax.dot_general(
+            x, turned, (((1,), (1,)), ((), ())), preferred_element_type=jnp.float32
+        )
 
     def feed_forward(current, row_in, row_out):
         normed = gathered_norm(current, row_in)
-        gate_vals = jnp.dot(normed, gate_whole, preferred_element_type=jnp.float32)
-        upward = jnp.dot(normed, up_whole, preferred_element_type=jnp.float32)
+        both = jnp.dot(normed, both_whole, preferred_element_type=jnp.float32)
+        gate_vals, upward = both[:, :units], both[:, units:]
         hidden = (jax.nn.silu(gate_vals) * upward).astype(jnp.bfloat16)
-        partials = jnp.dot(hidden, down_whole, preferred_element_type=jnp.float32)
-        return settle(current, partials, row_out, 0.5)
+        return settle(current, onto(hidden, down_whole[:, :units]), row_out, 0.5)
 
     first = feed_forward(stream, 0, 1)
     normed_mix = gathered_norm(first, 2)
     local_rows = normed_mix.shape[0]
-
-    def fold_rows(block_rows):
-        return jnp.dot(normed_mix, block_rows, preferred_element_type=jnp.float32)
-
-    inner = fold_rows(collect(w_inner, "fs", 0))
-    bgate = fold_rows(collect(w_bgate, "fs", 0))
-    cgate = fold_rows(collect(w_cgate, "fs", 0))
+    mix_in = jnp.dot(normed_mix, mix_whole[:, : 3 * channels], preferred_element_type=jnp.float32)
+    inner, bgate, cgate = (mix_in[:, i * channels : (i + 1) * channels] for i in range(3))
     conv_input = cgate * inner
     earlier = from_behind(conv_input[local_rows - (TAPS - 1) :], "fs", 1)
     padded = jnp.concatenate([earlier, conv_input], axis=0)
@@ -107,8 +261,7 @@
     for tap in range(1, TAPS):
         conv = conv + conv_taps[tap] * padded[tap : tap + local_rows]
     gated = (bgate * conv).astype(jnp.bfloat16)
-    mix_partials = jnp.dot(gated, collect(w_out, "fs", 1), preferred_element_type=jnp.float32)
-    second = settle(first, mix_partials, 3, 1.0)
+    second = settle(first, onto(gated, mix_whole[:, 3 * channels :]), 3, 1.0)
     return feed_forward(second, 4, 5)
 
 

time: 522 us -> 242 us (0.46)
  waiting for transfers between devices: 267 us -> 29.6 us
  blocking collectives: 155 us -> 73.8 us
  Pallas kernels: 0 us -> 78 us
  between operations: 13.7 us -> 0.33 us
  matrix products: 25 us -> 12.6 us
  starting transfers between devices: 43.7 us -> 32.8 us
    all_gather x1 -> x0, waiting for transfers between devices: 186 us -> none  [rows_first(): whole, at, done = (lax.all_gather(both, axis, axis=0, tiled=True), 0, [])]
    pallas_call x0 -> x1, Pallas kernels: none -> 78 us  [gathered_weights(): pl.pallas_call(kernel, out_shape=[jax.ShapeDtypeStruct((ROWS * Z_LO * Y,...]
    all_to_all x6 -> x4, waiting for transfers between devices: 81.2 us -> 13.9 us  [from_everyone(): return lax.all_to_all(copies, axis, split_axis=0, concat_axis=0, tiled=True)]
    all_to_all x3 -> x2, blocking collectives: 81.1 us -> 37.6 us  [sent_and_summed(): lax.all_to_all(parts, axis, split_axis=0, concat_axis=0, tiled=True)]
    all_to_all x4 -> x2, blocking collectives: 74.4 us -> 36.1 us  [from_everyone(): return lax.all_to_all(copies, axis, split_axis=0, concat_axis=0, tiled=True)]
    all_to_all x6 -> x4, starting transfers between devices: 40.6 us -> 23 us  [from_everyone(): return lax.all_to_all(copies, axis, split_axis=0, concat_axis=0, tiled=True)]
    all_to_all x0 -> x1, waiting for transfers between devices: none -> 15 us  [sent_and_summed(): lax.all_to_all(parts, axis, split_axis=0, concat_axis=0, tiled=True)]
    dot_general x7 -> x6, matrix products: 25 us -> 12.6 us  [the longest x2 9.29 us: feed_forward(): both = jnp.dot(normed, both_whole, preferred_element_type=jnp.float32)]
  transfers between devices with their start and end apart: 8 -> 6, of which waited for: 6 -> 5; matrix products, arithmetic and copies ran while one was open for 4% -> 1% of each run, Pallas kernels for 0% -> 33%
where the time goes in v1:
time: 242 us; the launch traced here: 239 us
  Pallas kernels  78 us (32%)
  blocking collectives  73.8 us (30%)
  starting transfers between devices  32.8 us (14%)
  waiting for transfers between devices  29.6 us (12%)
  matrix products  12.6 us (5%)
  local copies, waits for them, and re-layouts  7.16 us (3%)
  other arithmetic  5.25 us (2%)
    pallas_call x1, Pallas kernels, gathered_weights(): pl.pallas_call(kernel, out_shape=[jax.ShapeDtypeStruct((ROWS * Z_LO * Y,...  78 us
    all_to_all x2, blocking collectives, sent_and_summed(): lax.all_to_all(parts, axis, split_axis=0, concat_axis=0, tiled=True)  37.6 us
    all_to_all x2, blocking collectives, from_everyone(): return lax.all_to_all(copies, axis, split_axis=0, concat_axis=0, tiled=True)  36.1 us
    all_to_all x4, starting transfers between devices, from_everyone(): return lax.all_to_all(copies, axis, split_axis=0, concat_axis=0, tiled=True)  23 us
    all_to_all x1, waiting for transfers between devices, sent_and_summed(): lax.all_to_all(parts, axis, split_axis=0, concat_axis=0, tiled=True)  15 us
    all_to_all x4, waiting for transfers between devices, from_everyone(): return lax.all_to_all(copies, axis, split_axis=0, concat_axis=0, tiled=True)  13.9 us
    dot_general x2, matrix products, feed_forward(): both = jnp.dot(normed, both_whole, preferred_element_type=jnp.float32)  9.29 us
    all_to_all x1, starting transfers between devices, sent_and_summed(): lax.all_to_all(parts, axis, split_axis=0, concat_axis=0, tiled=True)  7.42 us
  transfers between devices with their start and end apart: 6, of which 5 were waited for; matrix products, arithmetic and copies ran while one was open for 1% of the time, Pallas kernels for 33%

profile of v1, /device:TPU:1, one launch (start us, length us, event | category | flops | bytes accessed | tf_op | source)
XLA Modules:
  0.0 239.5 jit_solution(7286103021094994007)
XLA Ops:
  0.0 0.0 copy-start.8
  0.0 0.0 copy-start.9
  0.0 1.1 copy.26
  1.2 0.0 copy-start.5
  1.2 1.0 broadcast_in_dim.12
  2.2 10.3 %all-to-all-start = ((bf16[8,256,256]{1,2,0:T(8,128)(2,1)}), bf16[8,256,256]{1,2,0:T(8,128)(2,1)S(1)}, u32[]{:S(2)}, u32[]{:S(2)}) async-start(bf16[8,256,256]{1,2,0:T(8,128)(2,1)} %broadcast_in_dim.12), calls=%async_computation | async-start | bytes 2097152 | tf_op jit(solution)/shard_map/all_to_all | solution.py:175
  12.5 0.0 copy-done.2
  12.5 0.7 pad.4.refs_1_
  13.1 0.0 copy-done.8
  13.1 0.6 pad_maximum_fusion.2.refs_2_
  13.8 0.0 copy-done.4
  13.8 0.8 pad_maximum_fusion.refs_0_
  14.5 78.0 %shard_map.100 = (bf16[2048,1408]{1,0:T(8,128)(2,1)}, bf16[2048,768]{1,0:T(8,128)(2,1)}, bf16[2048,512]{1,0:T(8,128)(2,1)}) custom-call(bf16[64,1408]{1,0:T(8,128)(2,1)} %pad_maximum_fusion.refs_0_, bf16[64,768]{1,0:T(8,128)(2,1)} %pad.4.refs_1_, bf16[64,512]{1,0:T(8,128)(2,1)} %pad_maximum_fusion.2.refs_2_), custom_call_target="tpu_custom_call" | custom-call | tf_op jit(solution)/shard_map/pallas_call | solution.py:154
  92.6 0.0 all-to-all-done
  92.6 0.3 multiply_reduce_fusion.2
  93.0 0.3 fusion.15
  93.3 0.0 copy-start.11
  93.3 4.6 %fusion.40 = f32[256,1408]{1,0:T(8,128)S(1)} fusion(bf16[256,2048]{0,1:T(8,128)(2,1)S(1)} %fusion.15, bf16[2048,1408]{1,0:T(8,128)(2,1)} %get-tuple-element.8), kind=kOutput, calls=%fused_computation.72 | convolution fusion | flops 1476395008 | bytes 8257536 | tf_op jit(solution)/shard_map/dot_general | solution.py:247
  98.0 0.0 copy-done.11
  98.0 1.0 fusion.4
  99.0 1.0 copy.46
  100.1 7.4 %all-to-all-start.1 = ((bf16[8,256,256]{2,1,0:T(8,128)(2,1)}), bf16[8,256,256]{2,1,0:T(8,128)(2,1)S(1)}, u32[]{:S(2)}, u32[]{:S(2)}) async-start(bf16[8,256,256]{2,1,0:T(8,128)(2,1)} %bitcast.63), calls=%async_computation.1 | async-start | bytes 2097152 | tf_op jit(solution)/shard_map/all_to_all | solution.py:190
  107.5 15.0 %all-to-all-done.1 = bf16[8,256,256]{2,1,0:T(8,128)(2,1)S(1)} async-done(((bf16[8,256,256]{2,1,0:T(8,128)(2,1)}), bf16[8,256,256]{2,1,0:T(8,128)(2,1)S(1)}, u32[]{:S(2)}, u32[]{:S(2)}) %all-to-all-start.1) | async-done | bytes 1048608 | tf_op jit(solution)/shard_map/all_to_all | solution.py:190
  122.5 0.1 convert_reduce_fusion.2
  122.6 0.1 multiply_reduce_fusion.5
  122.7 0.6 broadcast_in_dim.13
  123.3 4.2 %all-to-all-start.2 = ((f32[8,1,256]{2,1,0:T(1,128)}), f32[8,1,256]{2,1,0:T(1,128)S(1)}, u32[]{:S(2)}, u32[]{:S(2)}) async-start(f32[8,1,256]{2,1,0:T(1,128)} %broadcast_in_dim.13), calls=%async_computation.2 | async-start | bytes 16384 | tf_op jit(solution)/shard_map/all_to_all | solution.py:175
  127.5 4.6 %all-to-all-done.2 = f32[8,1,256]{2,1,0:T(1,128)S(1)} async-done(((f32[8,1,256]{2,1,0:T(1,128)}), f32[8,1,256]{2,1,0:T(1,128)S(1)}, u32[]{:S(2)}, u32[]{:S(2)}) %all-to-all-start.2) | async-done | bytes 8224 | tf_op jit(solution)/shard_map/all_to_all | solution.py:175
  132.2 0.1 add_convert_fusion.2
  132.3 0.1 copy.29
  132.4 0.1 broadcast_in_dim.14
  132.5 18.1 %all_to_all.48 = bf16[8,256,256]{1,2,0:T(8,128)(2,1)S(1)} all-to-all(bf16[8,256,256]{1,2,0:T(8,128)(2,1)S(1)} %broadcast_in_dim.14), channel_id=1, replica_groups=mesh['rep'=2,'fs'=32,'tp'=8] {'tp'}, dimensions={0} | all-to-all | bytes 2097152 | tf_op jit(solution)/shard_map/all_to_all | solution.py:175
  150.6 0.3 multiply_reduce_fusion.1
  150.9 0.3 fusion.13
  151.2 0.0 copy-start.10
  151.3 0.9 copy-done
  152.2 0.8 fusion.16
  153.0 2.4 %collective-permute-start = (f32[2,128]{1,0:T(2,128)S(1)}, f32[2,128]{1,0:T(2,128)S(1)}, u32[]{:S(2)}, u32[]{:S(2)}) collective-permute-start(f32[2,128]{1,0:T(2,128)S(1)} %slice.94), channel_id=1, source_target_pairs={{0,8},{8,16},{16,24},{24,32},{32,40},{40,48},{48,56},{56,64},{64,7... | collective-permute-start | bytes 3080 | tf_op jit(solution)/shard_map/ppermute | solution.py:202
  155.4 0.7 collective-permute-done
  156.1 0.5 convolution_convert_fusion
  156.5 0.1 copy.45
  156.6 19.2 %all_to_all.49 = bf16[8,256,256]{2,1,0:T(8,128)(2,1)S(1)} all-to-all(bf16[8,256,256]{2,1,0:T(8,128)(2,1)S(1)} %bitcast.65), channel_id=1, replica_groups=mesh['rep'=2,'fs'=32,'tp'=8] {'tp'}, dimensions={0} | all-to-all | bytes 2097152 | tf_op jit(solution)/shard_map/all_to_all | solution.py:190
  175.9 0.1 convert_reduce_fusion.1
  176.0 0.1 multiply_reduce_fusion.4
  176.1 0.6 broadcast_in_dim.30
  176.7 4.3 %all-to-all-start.5 = ((f32[8,1,256]{2,1,0:T(1,128)}), f32[8,1,256]{2,1,0:T(1,128)S(1)}, u32[]{:S(2)}, u32[]{:S(2)}) async-start(f32[8,1,256]{2,1,0:T(1,128)} %broadcast_in_dim.30), calls=%async_computation.5 | async-start | bytes 16384 | tf_op jit(solution)/shard_map/all_to_all | solution.py:175
  181.0 4.6 %all-to-all-done.5 = f32[8,1,256]{2,1,0:T(1,128)S(1)} async-done(((f32[8,1,256]{2,1,0:T(1,128)}), f32[8,1,256]{2,1,0:T(1,128)S(1)}, u32[]{:S(2)}, u32[]{:S(2)}) %all-to-all-start.5) | async-done | bytes 8224 | tf_op jit(solution)/shard_map/all_to_all | solution.py:175
  185.7 0.1 add_convert_fusion.1
  185.8 0.1 copy.32
  185.9 0.1 broadcast_in_dim.31
  186.0 18.1 %all_to_all.50 = bf16[8,256,256]{1,2,0:T(8,128)(2,1)S(1)} all-to-all(bf16[8,256,256]{1,2,0:T(8,128)(2,1)S(1)} %broadcast_in_dim.31), channel_id=1, replica_groups=mesh['rep'=2,'fs'=32,'tp'=8] {'tp'}, dimensions={0} | all-to-all | bytes 2097152 | tf_op jit(solution)/shard_map/all_to_all | solution.py:175
  204.0 0.3 multiply_reduce_fusion
  204.4 0.3 fusion.11
  204.7 0.0 copy-start.12
  204.7 4.6 %fusion.41 = f32[256,1408]{1,0:T(8,128)S(1)} fusion(bf16[256,2048]{0,1:T(8,128)(2,1)S(1)} %fusion.11, bf16[2048,1408]{1,0:T(8,128)(2,1)} %get-tuple-element.8), kind=kOutput, calls=%fused_computation.73 | convolution fusion | flops 1476395008 | bytes 8257536 | tf_op jit(solution)/shard_map/dot_general | solution.py:247
  209.4 1.0 fusion.7
  210.4 0.1 copy.44
  210.5 18.4 %all_to_all.51 = bf16[8,256,256]{2,1,0:T(8,128)(2,1)S(1)} all-to-all(bf16[8,256,256]{2,1,0:T(8,128)(2,1)S(1)} %bitcast.66), channel_id=1, replica_groups=mesh['rep'=2,'fs'=32,'tp'=8] {'tp'}, dimensions={0} | all-to-all | bytes 2097152 | tf_op jit(solution)/shard_map/all_to_all | solution.py:190
  228.9 0.1 convert_reduce_fusion
  229.0 0.1 multiply_reduce_fusion.3
  229.1 0.6 broadcast_in_dim.32
  229.8 4.3 %all-to-all-start.8 = ((f32[8,1,256]{2,1,0:T(1,128)}), f32[8,1,256]{2,1,0:T(1,128)S(1)}, u32[]{:S(2)}, u32[]{:S(2)}) async-start(f32[8,1,256]{2,1,0:T(1,128)} %broadcast_in_dim.32), calls=%async_computation.8 | async-start | bytes 16384 | tf_op jit(solution)/shard_map/all_to_all | solution.py:175
  234.0 4.6 %all-to-all-done.8 = f32[8,1,256]{2,1,0:T(1,128)S(1)} async-done(((f32[8,1,256]{2,1,0:T(1,128)}), f32[8,1,256]{2,1,0:T(1,128)S(1)}, u32[]{:S(2)}, u32[]{:S(2)}) %all-to-all-start.8) | async-done | bytes 8224 | tf_op jit(solution)/shard_map/all_to_all | solution.py:175
  238.7 0.8 add_convert_fusion
  (31 shorter events, 0.2 us)
Async XLA Ops:
  0.0 12.5 %copy-start.2 = (bf16[704,64]{0,1:T(8,128)(2,1)S(1)}, bf16[704,64]{0,1:T(8,128)(2,1)}, u32[]{:S(2)}) copy-start(bf16[704,64]{0,1:T(8,128)(2,1)} %param.14) | copy-start | bytes 270340
  0.0 13.1 %copy-start.6 = (bf16[128,64]{0,1:T(8,128)(2,1)S(1)}, bf16[128,64]{0,1:T(8,128)(2,1)}, u32[]{:S(2)}) copy-start(bf16[128,64]{0,1:T(8,128)(2,1)} %param.19) | copy-start | bytes 49156
  0.0 13.1 %copy-start.7 = (bf16[64,128]{1,0:T(8,128)(2,1)S(1)}, bf16[64,128]{1,0:T(8,128)(2,1)}, u32[]{:S(2)}) copy-start(bf16[64,128]{1,0:T(8,128)(2,1)} %param.17) | copy-start | bytes 49156
  0.0 13.1 %copy-start.8 = (bf16[64,128]{1,0:T(8,128)(2,1)S(1)}, bf16[64,128]{1,0:T(8,128)(2,1)}, u32[]{:S(2)}) copy-start(bf16[64,128]{1,0:T(8,128)(2,1)} %param.16) | copy-start | bytes 49156
  0.0 13.1 %copy-start.9 = (bf16[64,128]{1,0:T(8,128)(2,1)S(1)}, bf16[64,128]{1,0:T(8,128)(2,1)}, u32[]{:S(2)}) copy-start(bf16[64,128]{1,0:T(8,128)(2,1)} %param.15) | copy-start | bytes 49156
  0.0 13.7 %copy-start.3 = (bf16[64,704]{1,0:T(8,128)(2,1)S(1)}, bf16[64,704]{1,0:T(8,128)(2,1)}, u32[]{:S(2)}) copy-start(bf16[64,704]{1,0:T(8,128)(2,1)} %param.13) | copy-start | bytes 270340
  0.0 13.7 %copy-start.4 = (bf16[64,704]{1,0:T(8,128)(2,1)S(1)}, bf16[64,704]{1,0:T(8,128)(2,1)}, u32[]{:S(2)}) copy-start(bf16[64,704]{1,0:T(8,128)(2,1)} %param.12) | copy-start | bytes 270340
  1.2 91.4 %copy-start.5 = (f32[6,2048]{1,0:T(8,128)S(1)}, f32[6,2048]{1,0:T(8,128)}, u32[]{:S(2)}) copy-start(f32[6,2048]{1,0:T(8,128)} %param.11) | copy-start | bytes 147460
  2.2 90.4 %all-to-all-start = ((bf16[8,256,256]{1,2,0:T(8,128)(2,1)}), bf16[8,256,256]{1,2,0:T(8,128)(2,1)S(1)}, u32[]{:S(2)}, u32[]{:S(2)}) async-start(bf16[8,256,256]{1,2,0:T(8,128)(2,1)} %broadcast_in_dim.12), calls=%async_computation | async-start | bytes 2097152 | tf_op jit(solution)/shard_map/all_to_all | solution.py:175
  93.3 4.7 %copy-start.11 = (bf16[2048,768]{1,0:T(8,128)(2,1)S(1)}, bf16[2048,768]{1,0:T(8,128)(2,1)}, u32[]{:S(2)}) copy-start(bf16[2048,768]{1,0:T(8,128)(2,1)} %get-tuple-element.9) | copy-start | bytes 9437188
  100.1 32.1 %copy-start.1 = (bf16[256,256]{1,0:T(8,128)(2,1)S(1)}, bf16[256,256]{1,0:T(8,128)(2,1)}, u32[]{:S(2)}) copy-start(bf16[256,256]{1,0:T(8,128)(2,1)} %param.10) | copy-start | bytes 393220
  100.1 22.4 %all-to-all-start.1 = ((bf16[8,256,256]{2,1,0:T(8,128)(2,1)}), bf16[8,256,256]{2,1,0:T(8,128)(2,1)S(1)}, u32[]{:S(2)}, u32[]{:S(2)}) async-start(bf16[8,256,256]{2,1,0:T(8,128)(2,1)} %bitcast.63), calls=%async_computation.1 | async-start | bytes 2097152 | tf_op jit(solution)/shard_map/all_to_all | solution.py:190
  123.3 8.8 %all-to-all-start.2 = ((f32[8,1,256]{2,1,0:T(1,128)}), f32[8,1,256]{2,1,0:T(1,128)S(1)}, u32[]{:S(2)}, u32[]{:S(2)}) async-start(f32[8,1,256]{2,1,0:T(1,128)} %broadcast_in_dim.13), calls=%async_computation.2 | async-start | bytes 16384 | tf_op jit(solution)/shard_map/all_to_all | solution.py:175
  150.6 1.6 copy-start
  151.2 4.1 %copy-start.10 = (f32[3,128]{1,0:T(4,128)S(1)}, f32[3,128]{1,0:T(4,128)}, u32[]{:S(2)}) copy-start(f32[3,128]{1,0:T(4,128)} %param.18) | copy-start | bytes 4612
  153.0 3.1 %collective-permute-start = (f32[2,128]{1,0:T(2,128)S(1)}, f32[2,128]{1,0:T(2,128)S(1)}, u32[]{:S(2)}, u32[]{:S(2)}) collective-permute-start(f32[2,128]{1,0:T(2,128)S(1)} %slice.94), channel_id=1, source_target_pairs={{0,8},{8,16},{16,24},{24,32},{32,40},{40,48},{48,56},{56,64},{64,7... | collective-permute-start | bytes 3080 | tf_op jit(solution)/shard_map/ppermute | solution.py:202
  176.7 8.9 %all-to-all-start.5 = ((f32[8,1,256]{2,1,0:T(1,128)}), f32[8,1,256]{2,1,0:T(1,128)S(1)}, u32[]{:S(2)}, u32[]{:S(2)}) async-start(f32[8,1,256]{2,1,0:T(1,128)} %broadcast_in_dim.30), calls=%async_computation.5 | async-start | bytes 16384 | tf_op jit(solution)/shard_map/all_to_all | solution.py:175
  204.7 4.7 %copy-start.12 = (bf16[2048,768]{1,0:T(8,128)(2,1)S(1)}, bf16[2048,768]{1,0:T(8,128)(2,1)}, u32[]{:S(2)}) copy-start(bf16[2048,768]{1,0:T(8,128)(2,1)} %get-tuple-element.9) | copy-start | bytes 9437188
  229.8 8.9 %all-to-all-start.8 = ((f32[8,1,256]{2,1,0:T(1,128)}), f32[8,1,256]{2,1,0:T(1,128)S(1)}, u32[]{:S(2)}, u32[]{:S(2)}) async-start(f32[8,1,256]{2,1,0:T(1,128)} %broadcast_in_dim.32), calls=%async_computation.8 | async-start | bytes 16384 | tf_op jit(solution)/shard_map/all_to_all | solution.py:175

commit v2 on v1

v2 whole, which is shorter than its diff:
```python
import jax
import jax.numpy as jnp
from jax import lax
from jax.experimental import pallas as pl
from jax.experimental.pallas import tpu as pltpu
from jax.sharding import PartitionSpec as P

TAPS = 3
EPSILON = 1e-06
Z_LO, Z_ALL, Y = 8, 16, 4
ROWS = 64
PARTS = (
    ((0, 640, "y"), (640, 768, "z")),
    ((0, 256, "y"), (256, 512, "z")),
    ((0, 128, "y"), (128, 384, "z")),
)
WIDTHS = (1408, 768, 512)
RATE = 46.6e3
HOP = 2.0
AHEAD = 4.0
X_COPIES = 9 * 3 + 10 * 3 + 8


class Copy:
    def __init__(self, number, part, link, dz, dy, row, rows, after):
        self.number, self.part, self.link = number, part, link
        self.dz, self.dy, self.row, self.rows = dz, dy, row, rows
        self.after, self.tail = after, 0.0
        stream, index = part
        self.time = rows * PARTS[stream][index][1] * 2 / RATE
        self.start = None


def all_copies():
    copies = []

    def add(part, link, dz, dy, after, row=0, rows=ROWS):
        copies.append(Copy(len(copies), part, link, dz, dy, row, rows, list(after)))
        return copies[-1]

    half = ROWS // 2
    for stream, parts in enumerate(PARTS):
        for index, (_, _, first) in enumerate(parts):
            part = (stream, index)

            def along_z(dy, own):
                came = {0: own}
                for sign, link, row in ((-1, "z+", 0), (1, "z-", half)):
                    previous = own
                    for step in range(3):
                        previous = [add(part, link, sign * step, dy, previous)]
                        came[sign * (step + 1)] = previous
                    last = add(part, link, sign * 3, dy, previous, row, half)
                    came.setdefault(4, []).append(last)
                return came

            def along_y(dz, own):
                up = add(part, "y+", dz, 0, own)
                down = add(part, "y-", dz, 0, own)
                far = [
                    add(part, "y+", dz, -1, [up], 0, half),
                    add(part, "y-", dz, 1, [down], half, half),
                ]
                return {0: own, -1: [up], 1: [down], 2: far}

            if first == "y":
                for dy, got in along_y(0, []).items():
                    along_z(dy, got)
            else:
                for dz, got in along_z(0, []).items():
                    along_y(dz, got)
    for copy in reversed(copies):
        for before in copy.after:
            before.tail = max(before.tail, copy.tail + copy.time + HOP)
    return copies


def planned():
    copies = all_copies()
    free = dict.fromkeys(("y+", "y-", "z+", "z-"), 0.0)
    waiting, flying, here, order, now = list(copies), [], set(), [], 0.0
    while waiting or flying:
        ready = [c for c in waiting if all(b.number in here for b in c.after)]
        ready.sort(key=lambda c: (c.part[0], -c.tail, c.number))
        for copy in ready:
            if free[copy.link] < now + AHEAD:
                free[copy.link] = max(free[copy.link], now) + copy.time
                flying.append((free[copy.link] + HOP, copy.number, copy))
                waiting.remove(copy)
                order.append(("start", copy, now))
        flying.sort(key=lambda f: f[:2])
        now, _, copy = flying.pop(0)
        here.add(copy.number)
        order.append(("wait", copy, now))
    return order, copies


MESH = pl.DeviceIdType.MESH
TOK, D, SLOTS, SLICE = 256, 2048, 8, 256
UNITS, CHANNELS = 704, 128
F32, BF16 = jnp.float32, jnp.bfloat16


def turned_dot(x, turned):
    return lax.dot_general(x, turned, (((1,), (1,)), ((), ())), preferred_element_type=F32)


def layer_kernel(order, copies, refs):
    (stream, gains, own0, own1, own2, taps, out, full0, full1, full2, send_sem, recv_sem, x_send,
     x_recv, act, first, second, branch1, branch2, normed, hidden, acc, pair_out, pair_in, far_out,
     far_in, near_out, near_in, conv, halo_out, halo_in, sq_out, sq_in) = refs
    own, full = (own0, own1, own2), (full0, full1, full2)
    rep, fs, tp = lax.axis_index("rep"), lax.axis_index("fs"), lax.axis_index("tp")
    z_lo, y = fs // Y, lax.rem(fs, Y)
    z = rep * Z_LO + z_lo
    x, core = tp // 2, lax.rem(tp, 2)

    def at(z_to, y_to):
        return (z_to // Z_LO, lax.rem(z_to, Z_LO) * Y + y_to, tp)

    def peer(slot):
        return (rep, fs, slot)

    def slot_of(dx, dc=0):
        return lax.rem(x + dx, 4) * 2 + (core if dc == 0 else 1 - core)

    place = {
        "y+": at(z, lax.rem(y + 1, Y)),
        "y-": at(z, lax.rem(y + Y - 1, Y)),
        "z+": at(lax.rem(z + 1, Z_ALL), y),
        "z-": at(lax.rem(z + Z_ALL - 1, Z_ALL), y),
    }
    up, down, partner = peer(slot_of(1)), peer(slot_of(3)), peer(slot_of(0, 1))
    after = (z * Y + y + 1 + Z_ALL * Y) % (Z_ALL * Y)
    before = (z * Y + y - 1 + Z_ALL * Y) % (Z_ALL * Y)
    next_place = at(after // Y, lax.rem(after, Y))
    last_place = at(before // Y, lax.rem(before, Y))
    others = [peer(lax.rem(tp + i, SLOTS)) for i in range(1, SLOTS)]

    barrier = pltpu.get_barrier_semaphore()
    greeted = [*place.values(), *others, next_place, last_place]
    for device in greeted:
        pl.semaphore_signal(barrier, inc=1, device_id=device, device_id_type=MESH)
    pl.semaphore_wait(barrier, len(greeted))

    def remote(copy):
        stream_, index = copy.part
        column, width, _ = PARTS[stream_][index]
        columns = pl.ds(column, width)
        block = lax.rem(z_lo + copy.dz + Z_LO, Z_LO) * Y + lax.rem(y + copy.dy + Y, Y)
        rows = pl.ds(pl.multiple_of(block * ROWS, ROWS) + copy.row, copy.rows)
        target = full[stream_].at[rows, columns]
        source = target
        if copy.dz == 0 and copy.dy == 0:
            source = own[stream_].at[pl.ds(copy.row, copy.rows), columns]
        return pltpu.make_async_remote_copy(
            src_ref=source,
            dst_ref=target,
            send_sem=send_sem.at[copy.number],
            recv_sem=recv_sem.at[copy.number],
            device_id=place[copy.link],
            device_id_type=MESH,
        )

    events = list(order)

    def pump(until):
        while events and events[0][2] <= until:
            kind, copy, _ = events.pop(0)
            if kind == "start":
                remote(copy).start()
            else:
                remote(copy).wait_recv()

    sent = []

    def send(source, target, device):
        number = len(sent)
        copy = pltpu.make_async_remote_copy(
            src_ref=source,
            dst_ref=target,
            send_sem=x_send.at[number],
            recv_sem=x_recv.at[number],
            device_id=device,
            device_id_type=MESH,
        )
        copy.start()
        sent.append(copy)
        return copy

    def gather_x(buffer, source, pace=lambda step: None):
        half = TOK // 2
        low, high = pl.ds(0, half), pl.ds(half, half)
        mine, left, right, far = slot_of(0), slot_of(3), slot_of(1), slot_of(2)

        def same(ref, device):
            return send(ref, ref, device)

        from_left = send(source, buffer.at[mine], up)
        from_right = send(source, buffer.at[mine], down)
        pairs = [send(source, buffer.at[mine], partner)]
        pace(0)
        from_left.wait_recv()
        far_low = same(buffer.at[left, low], up)
        pairs.append(same(buffer.at[left], partner))
        from_right.wait_recv()
        far_high = same(buffer.at[right, high], down)
        pairs.append(same(buffer.at[right], partner))
        pace(1)
        far_low.wait_recv()
        pairs.append(same(buffer.at[far, low], partner))
        far_high.wait_recv()
        pairs.append(same(buffer.at[far, high], partner))
        pace(2)
        for copy in pairs:
            copy.wait_recv()

    def reduce_x(use, product):
        half = TOK // 2
        low, high = pl.ds(0, half), pl.ds(half, half)
        pair = {}
        for d in (2, 1, 3, 0):
            pair_out[use, d] = product(slot_of(d, 1)).astype(BF16)
            pair[d] = send(pair_out.at[use, d], pair_in.at[use, d], partner)
        for d in (2, 1, 3, 0):
            acc[d] = product(slot_of(d))

        def chip_sum(d, rows):
            return acc[d, rows] + pair_in[use, d, rows].astype(F32)

        pair[2].wait_recv()
        far_out[use, 0] = chip_sum(2, low).astype(BF16)
        far_low = send(far_out.at[use, 0], far_in.at[use, 0], up)
        far_out[use, 1] = chip_sum(2, high).astype(BF16)
        far_high = send(far_out.at[use, 1], far_in.at[use, 1], down)
        pair[1].wait_recv()
        near_out[use, 0, high] = chip_sum(1, high).astype(BF16)
        near = [send(near_out.at[use, 0, high], near_in.at[use, 0, high], up)]
        pair[3].wait_recv()
        near_out[use, 1, low] = chip_sum(3, low).astype(BF16)
        near.append(send(near_out.at[use, 1, low], near_in.at[use, 1, low], down))
        pair[0].wait_recv()
        far_low.wait_recv()
        near_out[use, 0, low] = (chip_sum(1, low) + far_in[use, 0].astype(F32)).astype(BF16)
        near.append(send(near_out.at[use, 0, low], near_in.at[use, 0, low], up))
        far_high.wait_recv()
        near_out[use, 1, high] = (chip_sum(3, high) + far_in[use, 1].astype(F32)).astype(BF16)
        near.append(send(near_out.at[use, 1, high], near_in.at[use, 1, high], down))
        for copy in near:
            copy.wait_recv()
        total = acc[0] + pair_in[use, 0].astype(F32)
        return total + near_in[use, 0].astype(F32) + near_in[use, 1].astype(F32)

    def scale_of(squares):
        return lax.rsqrt(squares / D + EPSILON)

    def squares_of(values):
        return jnp.sum(values * values, axis=1, keepdims=True)

    def normalize(buffer, row):
        squares = jnp.zeros((TOK, 1), F32)
        for j in range(SLOTS):
            squares = squares + squares_of(buffer[j].astype(F32))
        scale = scale_of(squares)
        for j in range(SLOTS):
            values = buffer[j].astype(F32) * scale * gains[row, j]
            normed[:, j * SLICE : (j + 1) * SLICE] = values.astype(BF16)

    def settle(current, branch, row, weight, result):
        squares = jnp.zeros((TOK, 1), F32)
        for j in range(SLOTS):
            squares = squares + squares_of(branch[j].astype(F32))
        scale = scale_of(squares)
        for j in range(SLOTS):
            step = branch[j].astype(F32) * scale * gains[row, j]
            result[j] = (current[j].astype(F32) + weight * step).astype(BF16)

    def silu(v):
        return v / (1.0 + jnp.exp(-v))

    def gate_and_up():
        def block(i, _):
            columns = pl.ds(pl.multiple_of(i * 256, 256), 256)
            both = jnp.dot(normed[...], full0[:, columns], preferred_element_type=F32)
            value = silu(both[:, :128]) * both[:, 128:]
            hidden[:, pl.ds(pl.multiple_of(i * 128, 128), 128)] = value.astype(BF16)
            return 0

        lax.fori_loop(0, 5, block, 0)
        both = jnp.dot(normed[...], full0[:, 1280:1408], preferred_element_type=F32)
        value = silu(both) * pltpu.roll(both, 64, 1)
        lane = lax.broadcasted_iota(jnp.int32, value.shape, 1)
        hidden[:, 640:768] = jnp.where(lane < 64, value, 0.0).astype(BF16)

    def slot_rows(slot):
        return pl.ds(pl.multiple_of(slot * SLICE, SLICE), SLICE)

    def down_product(slot):
        return turned_dot(hidden[...], full1[slot_rows(slot), :])

    act[tp] = stream[...]
    mine = pl.ds(pl.multiple_of(fs * ROWS, ROWS), ROWS)
    pump(0.0)
    for s in range(3):
        full[s][mine, :] = own[s][...]
    gather_x(act, stream, lambda step: pump((3.0, 6.0, 9.0)[step]))
    normalize(act, 0)
    both_here = max(t for kind, c, t in order if kind == "wait" and c.part[0] == 0)
    pump(both_here)
    gate_and_up()
    pump(1e9)

    branch1[tp] = reduce_x(0, down_product).astype(BF16)
    gather_x(branch1, branch1.at[tp])
    settle(act, branch1, 1, 0.5, first)

    normalize(first, 2)
    mix_in = jnp.dot(normed[...], full2[:, : 3 * CHANNELS], preferred_element_type=F32)
    conv_input = mix_in[:, 2 * CHANNELS :] * mix_in[:, :CHANNELS]
    conv[8:] = conv_input
    halo_out[...] = conv_input[TOK - 8 :]
    halo = send(halo_out, halo_in, next_place)
    halo.wait_recv()
    conv[:8] = jnp.where(fs == 0, 0.0, halo_in[...])
    mixed = taps[0:1, :] * conv[6 : 6 + TOK]
    for tap in range(1, TAPS):
        mixed = mixed + taps[tap : tap + 1, :] * conv[6 + tap : 6 + tap + TOK]
    hidden[:, :CHANNELS] = (mix_in[:, CHANNELS : 2 * CHANNELS] * mixed).astype(BF16)

    def out_product(slot):
        return turned_dot(hidden[:, :CHANNELS], full2[slot_rows(slot), 3 * CHANNELS :])

    branch2[tp] = reduce_x(1, out_product).astype(BF16)
    gather_x(branch2, branch2.at[tp])
    settle(first, branch2, 3, 1.0, second)

    normalize(second, 4)
    gate_and_up()
    branch = reduce_x(2, down_product)
    squares = jnp.broadcast_to(squares_of(branch), (TOK, 128))
    sq_out[...] = jnp.transpose(squares)[:8]
    got = [send(sq_out, sq_in.at[i], device) for i, device in enumerate(others)]
    total = sq_out[...]
    for copy in got:
        copy.wait_recv()
    for i in range(SLOTS - 1):
        total = total + sq_in[i]
    scale = jnp.transpose(scale_of(jnp.concatenate([total] * 16, axis=0)))[:, :1]
    step = branch * scale * gains[5, tp]
    out[...] = (second[tp].astype(F32) + 0.5 * step).astype(BF16)

    for copy in copies:
        remote(copy).wait_send()
    for copy in sent:
        copy.wait_send()


def whole_layer(stream, gains, pieces, taps):
    order, copies = planned()

    def kernel(*refs):
        layer_kernel(order, copies, refs)

    slots = (SLOTS, TOK, SLICE)
    half = TOK // 2
    scratch = [pltpu.VMEM((ROWS * Z_LO * Y, w), BF16) for w in WIDTHS]
    scratch += [pltpu.SemaphoreType.DMA((len(copies),))] * 2
    scratch += [pltpu.SemaphoreType.DMA((X_COPIES,))] * 2
    scratch += [pltpu.VMEM(slots, BF16)] * 5
    scratch += [
        pltpu.VMEM((TOK, D), BF16),
        pltpu.VMEM((TOK, 768), BF16),
        pltpu.VMEM((4, TOK, SLICE), F32),
        pltpu.VMEM((3, 4, TOK, SLICE), BF16),
        pltpu.VMEM((3, 4, TOK, SLICE), BF16),
        pltpu.VMEM((3, 2, half, SLICE), BF16),
        pltpu.VMEM((3, 2, half, SLICE), BF16),
        pltpu.VMEM((3, 2, TOK, SLICE), BF16),
        pltpu.VMEM((3, 2, TOK, SLICE), BF16),
        pltpu.VMEM((TOK + 8, CHANNELS), F32),
        pltpu.VMEM((8, CHANNELS), F32),
        pltpu.VMEM((8, CHANNELS), F32),
        pltpu.VMEM((8, TOK), F32),
        pltpu.VMEM((SLOTS - 1, 8, TOK), F32),
    ]
    return pl.pallas_call(
        kernel,
        out_shape=jax.ShapeDtypeStruct(stream.shape, BF16),
        in_specs=[pl.BlockSpec(memory_space=pltpu.VMEM)] * 6,
        out_specs=pl.BlockSpec(memory_space=pltpu.VMEM),
        scratch_shapes=scratch,
        compiler_params=pltpu.CompilerParams(
            collective_id=0, has_side_effects=True, vmem_limit_bytes=60 * 2**20
        ),
    )(stream, gains, *pieces, taps)


def packed(w_gate, w_up, w_down, w_inner, w_bgate, w_cgate, w_out):
    blocks = []
    for at in range(0, UNITS, 128):
        blocks += [w_gate[:, at : at + 128], w_up[:, at : at + 128]]
    first = jnp.concatenate(blocks, axis=1)
    second = jnp.pad(w_down.T, ((0, 0), (0, 64)))
    third = jnp.concatenate([w_inner, w_bgate, w_cgate, w_out.T], axis=1)
    return first, second, third


def shards(stream, norm_gains, w_gate, w_up, w_down, w_inner, w_bgate, w_cgate, conv_taps, w_out):
    pieces = packed(w_gate, w_up, w_down, w_inner, w_bgate, w_cgate, w_out)
    gains = norm_gains.reshape(-1, SLOTS, 1, SLICE)
    return whole_layer(stream, gains, pieces, conv_taps)


def solution(mesh):
    return jax.shard_map(
        shards,
        mesh=mesh,
        in_specs=(
            P(("rep", "fs"), "tp"),
            P(),
            P("fs", "tp"),
            P("fs", "tp"),
            P("tp", "fs"),
            P("fs", "tp"),
            P("fs", "tp"),
            P("fs", "tp"),
            P(None, "tp"),
            P("tp", "fs"),
        ),
        out_specs=P(("rep", "fs"), "tp"),
        check_vma=False,
    )
```

time: 242 us -> 155 us (0.64)
  blocking collectives: 73.8 us -> 0 us
  Pallas kernels: 78 us -> 148 us
  starting transfers between devices: 32.8 us -> 0 us
  waiting for transfers between devices: 29.6 us -> 0 us
  matrix products: 12.6 us -> 0 us
  other arithmetic: 5.25 us -> 0.62 us
    all_to_all x4 -> x0, blocking collectives: 73.8 us -> none  [the longest x2 37.6 us: sent_and_summed(): lax.all_to_all(parts, axis, split_axis=0, concat_axis=0, tiled=True)]
    pallas_call x1, Pallas kernels: 78 us -> 148 us  [whole_layer(): pl.pallas_call(kernel, out_shape=jax.ShapeDtypeStruct(stream.shape, BF16)...]
    all_to_all x5 -> x0, starting transfers between devices: 30.4 us -> none  [the longest x4 23 us: from_everyone(): return lax.all_to_all(copies, axis, split_axis=0, concat_axis=0, tiled=True)]
    all_to_all x5 -> x0, waiting for transfers between devices: 28.9 us -> none  [the longest x1 15 us: sent_and_summed(): lax.all_to_all(parts, axis, split_axis=0, concat_axis=0, tiled=True)]
    dot_general x6 -> x0, matrix products: 12.6 us -> none  [the longest x2 9.29 us: feed_forward(): both = jnp.dot(normed, both_whole, preferred_element_type=jnp.float32)]
    broadcast_in_dim x6 -> x0, local copies, waits for them, and re-layouts: 3.01 us -> none  [from_everyone(): copies = jnp.broadcast_to(x, (lax.axis_size(axis), *x.shape))]
  transfers between devices with their start and end apart: 6 -> 0, of which waited for: 5 -> 0; matrix products, arithmetic and copies ran while one was open for 1% -> 0% of each run, Pallas kernels for 33% -> 0%
where the time goes in v2:
time: 155 us
  Pallas kernels  148 us (95%)
  local copies, waits for them, and re-layouts  5.75 us (4%)
    pallas_call x1, Pallas kernels, whole_layer(): pl.pallas_call(kernel, out_shape=jax.ShapeDtypeStruct(stream.shape, BF16)...  148 us

profile of v2, /device:TPU:1, one launch (start us, length us, event | category | flops | bytes accessed | tf_op | source)
XLA Modules:
  0.0 154.9 jit_solution(4074258137223986586)
XLA Ops:
  0.0 0.9 fusion
  0.9 0.0 slice-start
  0.9 0.0 slice-start.1
  0.9 0.7 slice-done
  1.6 0.0 slice-done.1
  1.6 0.0 copy-start
  1.6 0.8 concatenate.6.refs_2_
  2.4 0.1 copy-done
  2.5 0.0 copy-start.2
  2.5 0.0 copy-start.3
  2.5 0.0 copy-start.4
  2.5 0.0 copy-start.5
  2.5 0.7 pad.4.refs_3_
  3.2 0.1 copy-done.2
  3.2 0.0 copy-done.3
  3.2 0.0 copy-done.4
  3.3 0.0 copy-done.5
  3.3 0.0 copy-start.1
  3.3 0.6 pad_maximum_fusion.refs_4_
  3.9 0.2 copy-done.1
  4.2 0.7 reshape.3.refs_1_
  4.8 148.5 %shard_map.100 = bf16[256,256]{1,0:T(8,128)(2,1)} custom-call(bf16[256,256]{1,0:T(8,128)(2,1)} %refs_0_.1, f32[6,8,1,256]{3,2,1,0:T(1,128)} %reshape.3.refs_1_, bf16[64,1408]{1,0:T(8,128)(2,1)} %concatenate.6.refs_2_, bf16[64,768]{1,0:T(8,128)(2,1)} %pad.4.refs_3_, bf16[64,512]{1,0:T(8,128)(2,1)} %pad_maximum_fusion.refs_4_, f32[3,128]{1,0:T(4,128)} %refs_5_.1), custom_call_target="tpu_custom_call" | custom-call | tf_op jit(solution)/shard_map/pallas_call | solution.py:386
  153.3 1.6 %copy.12 = bf16[256,256]{1,0:T(8,128)(2,1)} copy(bf16[256,256]{1,0:T(8,128)(2,1)} %shard_map.100) | data formatting | bytes 262144
Async XLA Ops:
  0.9 0.7 slice-start
  0.9 0.7 slice-start.1
  1.6 0.9 copy-start
  2.5 0.7 copy-start.2
  2.5 0.7 copy-start.3
  2.5 0.8 copy-start.4
  2.5 0.8 copy-start.5
  3.3 0.8 copy-start.1

commit v3 on v2

--- a/solution.py
+++ b/solution.py
@@ -10,14 +10,13 @@
 Z_LO, Z_ALL, Y = 8, 16, 4
 ROWS = 64
 PARTS = (
-    ((0, 640, "y"), (640, 768, "z")),
-    ((0, 256, "y"), (256, 512, "z")),
+    ((0, 896, "y"), (896, 1280, "z")),
     ((0, 128, "y"), (128, 384, "z")),
 )
-WIDTHS = (1408, 768, 512)
-RATE = 46.6e3
-HOP = 2.0
-AHEAD = 4.0
+WIDTHS = (2176, 512)
+RATE = 52e3
+HOP = 2.8
+AHEAD = 6.0
 X_COPIES = 9 * 3 + 10 * 3 + 8
 
 
@@ -106,10 +105,11 @@
 
 
 def layer_kernel(order, copies, refs):
-    (stream, gains, own0, own1, own2, taps, out, full0, full1, full2, send_sem, recv_sem, x_send,
-     x_recv, act, first, second, branch1, branch2, normed, hidden, acc, pair_out, pair_in, far_out,
-     far_in, near_out, near_in, conv, halo_out, halo_in, sq_out, sq_in) = refs
-    own, full = (own0, own1, own2), (full0, full1, full2)
+    (stream, gains, w_gate, w_up, w_down, w_inner, w_bgate, w_cgate, w_out, taps, out, full0, full1,
+     send_sem, recv_sem, x_send, x_recv, act, first, second, branch1, branch2, normed, hidden, acc,
+     pair_out, pair_in, far_out, far_in, near_out, near_in, conv, halo_out, halo_in, sq_out,
+     sq_in) = refs
+    full = (full0, full1)
     rep, fs, tp = lax.axis_index("rep"), lax.axis_index("fs"), lax.axis_index("tp")
     z_lo, y = fs // Y, lax.rem(fs, Y)
     z = rep * Z_LO + z_lo
@@ -137,6 +137,21 @@
     last_place = at(before // Y, lax.rem(before, Y))
     others = [peer(lax.rem(tp + i, SLOTS)) for i in range(1, SLOTS)]
 
+    mine = pl.ds(pl.multiple_of(fs * ROWS, ROWS), ROWS)
+    for i in range(5):
+        columns = slice(128 * i, 128 * i + 128)
+        full0[mine, 256 * i : 256 * i + 128] = w_gate[:, columns]
+        full0[mine, 256 * i + 128 : 256 * i + 256] = w_up[:, columns]
+    full0[mine, 1280:1408] = jnp.concatenate([w_gate[:, 640:], w_up[:, 640:]], axis=1)
+    full0[mine, 1408:2048] = w_down[:, :640]
+    rest = jnp.concatenate([w_down[:, 640:], jnp.zeros((ROWS, 64), BF16)], axis=1)
+    full0[mine, 2048:2176] = rest
+    full1[mine, :128] = w_inner[...]
+    full1[mine, 128:256] = w_bgate[...]
+    full1[mine, 256:384] = w_cgate[...]
+    full1[mine, 384:] = w_out[...]
+    act[tp] = stream[...]
+
     barrier = pltpu.get_barrier_semaphore()
     greeted = [*place.values(), *others, next_place, last_place]
     for device in greeted:
@@ -150,11 +165,8 @@
         block = lax.rem(z_lo + copy.dz + Z_LO, Z_LO) * Y + lax.rem(y + copy.dy + Y, Y)
         rows = pl.ds(pl.multiple_of(block * ROWS, ROWS) + copy.row, copy.rows)
         target = full[stream_].at[rows, columns]
-        source = target
-        if copy.dz == 0 and copy.dy == 0:
-            source = own[stream_].at[pl.ds(copy.row, copy.rows), columns]
         return pltpu.make_async_remote_copy(
-            src_ref=source,
+            src_ref=target,
             dst_ref=target,
             send_sem=send_sem.at[copy.number],
             recv_sem=recv_sem.at[copy.number],
@@ -215,15 +227,17 @@
         for copy in pairs:
             copy.wait_recv()
 
-    def reduce_x(use, product):
+    def reduce_x(use, product, pace=lambda step: None):
         half = TOK // 2
         low, high = pl.ds(0, half), pl.ds(half, half)
         pair = {}
         for d in (2, 1, 3, 0):
             pair_out[use, d] = product(slot_of(d, 1)).astype(BF16)
             pair[d] = send(pair_out.at[use, d], pair_in.at[use, d], partner)
+        pace(0)
         for d in (2, 1, 3, 0):
             acc[d] = product(slot_of(d))
+        pace(1)
 
         def chip_sum(d, rows):
             return acc[d, rows] + pair_in[use, d, rows].astype(F32)
@@ -233,6 +247,7 @@
         far_low = send(far_out.at[use, 0], far_in.at[use, 0], up)
         far_out[use, 1] = chip_sum(2, high).astype(BF16)
         far_high = send(far_out.at[use, 1], far_in.at[use, 1], down)
+        pace(2)
         pair[1].wait_recv()
         near_out[use, 0, high] = chip_sum(1, high).astype(BF16)
         near = [send(near_out.at[use, 0, high], near_in.at[use, 0, high], up)]
@@ -240,12 +255,14 @@
         near_out[use, 1, low] = chip_sum(3, low).astype(BF16)
         near.append(send(near_out.at[use, 1, low], near_in.at[use, 1, low], down))
         pair[0].wait_recv()
+        pace(3)
         far_low.wait_recv()
         near_out[use, 0, low] = (chip_sum(1, low) + far_in[use, 0].astype(F32)).astype(BF16)
         near.append(send(near_out.at[use, 0, low], near_in.at[use, 0, low], up))
         far_high.wait_recv()
         near_out[use, 1, high] = (chip_sum(3, high) + far_in[use, 1].astype(F32)).astype(BF16)
         near.append(send(near_out.at[use, 1, high], near_in.at[use, 1, high], down))
+        pace(4)
         for copy in near:
             copy.wait_recv()
         total = acc[0] + pair_in[use, 0].astype(F32)
@@ -263,7 +280,7 @@
             squares = squares + squares_of(buffer[j].astype(F32))
         scale = scale_of(squares)
         for j in range(SLOTS):
-            values = buffer[j].astype(F32) * scale * gains[row, j]
+            values = buffer[j].astype(F32) * scale * gains[row : row + 1, j * SLICE : (j + 1) * SLICE]
             normed[:, j * SLICE : (j + 1) * SLICE] = values.astype(BF16)
 
     def settle(current, branch, row, weight, result):
@@ -272,7 +289,7 @@
             squares = squares + squares_of(branch[j].astype(F32))
         scale = scale_of(squares)
         for j in range(SLOTS):
-            step = branch[j].astype(F32) * scale * gains[row, j]
+            step = branch[j].astype(F32) * scale * gains[row : row + 1, j * SLICE : (j + 1) * SLICE]
             result[j] = (current[j].astype(F32) + weight * step).astype(BF16)
 
     def silu(v):
@@ -296,26 +313,23 @@
         return pl.ds(pl.multiple_of(slot * SLICE, SLICE), SLICE)
 
     def down_product(slot):
-        return turned_dot(hidden[...], full1[slot_rows(slot), :])
-
-    act[tp] = stream[...]
-    mine = pl.ds(pl.multiple_of(fs * ROWS, ROWS), ROWS)
+        return turned_dot(hidden[...], full0[slot_rows(slot), 1408:])
+
     pump(0.0)
-    for s in range(3):
-        full[s][mine, :] = own[s][...]
     gather_x(act, stream, lambda step: pump((3.0, 6.0, 9.0)[step]))
     normalize(act, 0)
-    both_here = max(t for kind, c, t in order if kind == "wait" and c.part[0] == 0)
-    pump(both_here)
+    here = max(t for kind, c, t in order if kind == "wait" and c.part[0] == 0)
+    pump(here)
     gate_and_up()
-    pump(1e9)
-
-    branch1[tp] = reduce_x(0, down_product).astype(BF16)
-    gather_x(branch1, branch1.at[tp])
+    pump(here + 2.5)
+    branch1[tp] = reduce_x(
+        0, down_product, lambda step: pump(here + (3.3, 4.2, 5.0, 6.0, 9.5)[step])
+    ).astype(BF16)
+    gather_x(branch1, branch1.at[tp], lambda step: pump(here + (12.0, 16.0, 1e9)[step]))
     settle(act, branch1, 1, 0.5, first)
 
     normalize(first, 2)
-    mix_in = jnp.dot(normed[...], full2[:, : 3 * CHANNELS], preferred_element_type=F32)
+    mix_in = jnp.dot(normed[...], full1[:, : 3 * CHANNELS], preferred_element_type=F32)
     conv_input = mix_in[:, 2 * CHANNELS :] * mix_in[:, :CHANNELS]
     conv[8:] = conv_input
     halo_out[...] = conv_input[TOK - 8 :]
@@ -328,7 +342,7 @@
     hidden[:, :CHANNELS] = (mix_in[:, CHANNELS : 2 * CHANNELS] * mixed).astype(BF16)
 
     def out_product(slot):
-        return turned_dot(hidden[:, :CHANNELS], full2[slot_rows(slot), 3 * CHANNELS :])
+        return turned_dot(hidden[:, :CHANNELS], full1[slot_rows(slot), 3 * CHANNELS :])
 
     branch2[tp] = reduce_x(1, out_product).astype(BF16)
     gather_x(branch2, branch2.at[tp])
@@ -346,7 +360,7 @@
     for i in range(SLOTS - 1):
         total = total + sq_in[i]
     scale = jnp.transpose(scale_of(jnp.concatenate([total] * 16, axis=0)))[:, :1]
-    step = branch * scale * gains[5, tp]
+    step = branch * scale * gains[5:6, pl.ds(pl.multiple_of(tp * SLICE, SLICE), SLICE)]
     out[...] = (second[tp].astype(F32) + 0.5 * step).astype(BF16)
 
     for copy in copies:
@@ -355,7 +369,7 @@
         copy.wait_send()
 
 
-def whole_layer(stream, gains, pieces, taps):
+def whole_layer(*arrays):
     order, copies = planned()
 
     def kernel(*refs):
@@ -385,30 +399,20 @@
     ]
     return pl.pallas_call(
         kernel,
-        out_shape=jax.ShapeDtypeStruct(stream.shape, BF16),
-        in_specs=[pl.BlockSpec(memory_space=pltpu.VMEM)] * 6,
+        out_shape=jax.ShapeDtypeStruct(arrays[0].shape, BF16),
+        in_specs=[pl.BlockSpec(memory_space=pltpu.VMEM)] * len(arrays),
         out_specs=pl.BlockSpec(memory_space=pltpu.VMEM),
         scratch_shapes=scratch,
         compiler_params=pltpu.CompilerParams(
             collective_id=0, has_side_effects=True, vmem_limit_bytes=60 * 2**20
         ),
-    )(stream, gains, *pieces, taps)
-
-
-def packed(w_gate, w_up, w_down, w_inner, w_bgate, w_cgate, w_out):
-    blocks = []
-    for at in range(0, UNITS, 128):
-        blocks += [w_gate[:, at : at + 128], w_up[:, at : at + 128]]
-    first = jnp.concatenate(blocks, axis=1)
-    second = jnp.pad(w_down.T, ((0, 0), (0, 64)))
-    third = jnp.concatenate([w_inner, w_bgate, w_cgate, w_out.T], axis=1)
-    return first, second, third
+    )(*arrays)
 
 
 def shards(stream, norm_gains, w_gate, w_up, w_down, w_inner, w_bgate, w_cgate, conv_taps, w_out):
-    pieces = packed(w_gate, w_up, w_down, w_inner, w_bgate, w_cgate, w_out)
-    gains = norm_gains.reshape(-1, SLOTS, 1, SLICE)
-    return whole_layer(stream, gains, pieces, conv_taps)
+    return whole_layer(
+        stream, norm_gains, w_gate, w_up, w_down.T, w_inner, w_bgate, w_cgate, w_out.T, conv_taps
+    )
 
 
 def solution(mesh):

time: 155 us -> 149 us (0.961)
  local copies, waits for them, and re-layouts: 5.75 us -> 1.57 us
    slice x5 -> x0, local copies, waits for them, and re-layouts: 1.6 us -> none  [packed(): blocks += [w_gate[:, at:at + 128], w_up[:, at:at + 128]]]
where the time goes in v3:
time: 149 us
  Pallas kernels  147 us (99%)
  local copies, waits for them, and re-layouts  1.57 us (1%)
    pallas_call x1, Pallas kernels, whole_layer(): pl.pallas_call(kernel, out_shape=jax.ShapeDtypeStruct(arrays[0].shape, BF...  147 us

profile of v3, /device:TPU:1, one launch (start us, length us, event | category | flops | bytes accessed | tf_op | source)
XLA Modules:
  0.0 148.7 jit_solution(12124882017777525507)
XLA Ops:
  0.0 147.1 %shard_map.100 = bf16[256,256]{1,0:T(8,128)(2,1)} custom-call(bf16[256,256]{1,0:T(8,128)(2,1)} %refs_0_.1, f32[6,2048]{1,0:T(8,128)} %refs_1_.1, bf16[64,704]{1,0:T(8,128)(2,1)} %refs_2_.1, bf16[64,704]{1,0:T(8,128)(2,1)} %refs_3_.1, bf16[64,704]{1,0:T(8,128)(2,1)} %bitcast.2, bf16[64,128]{1,0:T(8,128)(2,1)} %refs_5_.1, bf16[64,128]{1,0:T(8,128)(2,1)} %refs_6_.1, ...), custom_call_target="tpu_custom_call" | custom-call | tf_op jit(solution)/shard_map/pallas_call | solution.py:400
  147.1 1.6 %copy.12 = bf16[256,256]{1,0:T(8,128)(2,1)} copy(bf16[256,256]{1,0:T(8,128)(2,1)} %shard_map.100) | data formatting | bytes 262144

commit v4 on v3

--- a/solution.py
+++ b/solution.py
@@ -16,8 +16,9 @@
 WIDTHS = (2176, 512)
 RATE = 52e3
 HOP = 2.8
-AHEAD = 6.0
-X_COPIES = 9 * 3 + 10 * 3 + 8
+AHEAD = (2.5, 2.5)
+LATER = 8
+X_COPIES = 13 * 3 + 10 * 3 + 8
 
 
 class Copy:
@@ -82,7 +83,9 @@
         ready = [c for c in waiting if all(b.number in here for b in c.after)]
         ready.sort(key=lambda c: (c.part[0], -c.tail, c.number))
         for copy in ready:
-            if free[copy.link] < now + AHEAD:
+            if copy.part[0] and sum(c.part[0] == 0 for c in waiting) > LATER:
+                break
+            if free[copy.link] < now + AHEAD[copy.part[0]]:
                 free[copy.link] = max(free[copy.link], now) + copy.time
                 flying.append((free[copy.link] + HOP, copy.number, copy))
                 waiting.remove(copy)
@@ -208,16 +211,24 @@
         def same(ref, device):
             return send(ref, ref, device)
 
-        from_left = send(source, buffer.at[mine], up)
-        from_right = send(source, buffer.at[mine], down)
+        near = {}
+        for rows_up, rows_down in ((low, high), (high, low)):
+            for key, rows, device in (("left", rows_up, up), ("right", rows_down, down)):
+                near.setdefault(key, []).append(
+                    send(source.at[rows], buffer.at[mine, rows], device)
+                )
         pairs = [send(source, buffer.at[mine], partner)]
         pace(0)
-        from_left.wait_recv()
+        near["left"][0].wait_recv()
         far_low = same(buffer.at[left, low], up)
-        pairs.append(same(buffer.at[left], partner))
-        from_right.wait_recv()
+        pairs.append(same(buffer.at[left, low], partner))
+        near["right"][0].wait_recv()
         far_high = same(buffer.at[right, high], down)
-        pairs.append(same(buffer.at[right], partner))
+        pairs.append(same(buffer.at[right, high], partner))
+        near["left"][1].wait_recv()
+        pairs.append(same(buffer.at[left, high], partner))
+        near["right"][1].wait_recv()
+        pairs.append(same(buffer.at[right, low], partner))
         pace(1)
         far_low.wait_recv()
         pairs.append(same(buffer.at[far, low], partner))
@@ -231,29 +242,36 @@
         half = TOK // 2
         low, high = pl.ds(0, half), pl.ds(half, half)
         pair = {}
-        for d in (2, 1, 3, 0):
+
+        def give(d):
             pair_out[use, d] = product(slot_of(d, 1)).astype(BF16)
             pair[d] = send(pair_out.at[use, d], pair_in.at[use, d], partner)
-        pace(0)
-        for d in (2, 1, 3, 0):
-            acc[d] = product(slot_of(d))
-        pace(1)
 
         def chip_sum(d, rows):
             return acc[d, rows] + pair_in[use, d, rows].astype(F32)
 
+        give(2)
+        acc[2] = product(slot_of(2))
+        give(1)
+        give(3)
+        give(0)
+        pace(0)
         pair[2].wait_recv()
         far_out[use, 0] = chip_sum(2, low).astype(BF16)
         far_low = send(far_out.at[use, 0], far_in.at[use, 0], up)
         far_out[use, 1] = chip_sum(2, high).astype(BF16)
         far_high = send(far_out.at[use, 1], far_in.at[use, 1], down)
-        pace(2)
+        pace(1)
+        acc[1] = product(slot_of(1))
         pair[1].wait_recv()
         near_out[use, 0, high] = chip_sum(1, high).astype(BF16)
         near = [send(near_out.at[use, 0, high], near_in.at[use, 0, high], up)]
+        acc[3] = product(slot_of(3))
         pair[3].wait_recv()
         near_out[use, 1, low] = chip_sum(3, low).astype(BF16)
         near.append(send(near_out.at[use, 1, low], near_in.at[use, 1, low], down))
+        acc[0] = product(slot_of(0))
+        pace(2)
         pair[0].wait_recv()
         pace(3)
         far_low.wait_recv()
@@ -321,11 +339,12 @@
     here = max(t for kind, c, t in order if kind == "wait" and c.part[0] == 0)
     pump(here)
     gate_and_up()
-    pump(here + 2.5)
+    pump(here + 2.0)
     branch1[tp] = reduce_x(
-        0, down_product, lambda step: pump(here + (3.3, 4.2, 5.0, 6.0, 9.5)[step])
+        0, down_product, lambda step: pump(here + (2.5, 3.5, 4.5, 5.5, 8.0)[step])
     ).astype(BF16)
-    gather_x(branch1, branch1.at[tp], lambda step: pump(here + (12.0, 16.0, 1e9)[step]))
+    gather_x(branch1, branch1.at[tp], lambda step: pump(here + (10.0, 14.5, 18.0)[step]))
+    pump(1e9)
     settle(act, branch1, 1, 0.5, first)
 
     normalize(first, 2)

time: 149 us -> 138 us (0.926)
  Pallas kernels: 147 us -> 136 us
    pallas_call x1, Pallas kernels: 147 us -> 136 us  [whole_layer(): pl.pallas_call(kernel, out_shape=jax.ShapeDtypeStruct(arrays[0].shape, BF...]
where the time goes in v4:
time: 138 us
  Pallas kernels  136 us (99%)
  local copies, waits for them, and re-layouts  1.57 us (1%)
    pallas_call x1, Pallas kernels, whole_layer(): pl.pallas_call(kernel, out_shape=jax.ShapeDtypeStruct(arrays[0].shape, BF...  136 us

profile of v4, /device:TPU:1, one launch (start us, length us, event | category | flops | bytes accessed | tf_op | source)
XLA Modules:
  0.0 138.0 jit_solution(12530801001082319291)
XLA Ops:
  0.0 136.4 %shard_map.100 = bf16[256,256]{1,0:T(8,128)(2,1)} custom-call(bf16[256,256]{1,0:T(8,128)(2,1)} %refs_0_.1, f32[6,2048]{1,0:T(8,128)} %refs_1_.1, bf16[64,704]{1,0:T(8,128)(2,1)} %refs_2_.1, bf16[64,704]{1,0:T(8,128)(2,1)} %refs_3_.1, bf16[64,704]{1,0:T(8,128)(2,1)} %bitcast.2, bf16[64,128]{1,0:T(8,128)(2,1)} %refs_5_.1, bf16[64,128]{1,0:T(8,128)(2,1)} %refs_6_.1, ...), custom_call_target="tpu_custom_call" | custom-call | tf_op jit(solution)/shard_map/pallas_call | solution.py:419
  136.4 1.6 %copy.12 = bf16[256,256]{1,0:T(8,128)(2,1)} copy(bf16[256,256]{1,0:T(8,128)(2,1)} %shard_map.100) | data formatting | bytes 262144

commit v5 on v4

--- a/solution.py
+++ b/solution.py
@@ -135,11 +135,13 @@
     }
     up, down, partner = peer(slot_of(1)), peer(slot_of(3)), peer(slot_of(0, 1))
     after = (z * Y + y + 1 + Z_ALL * Y) % (Z_ALL * Y)
-    before = (z * Y + y - 1 + Z_ALL * Y) % (Z_ALL * Y)
     next_place = at(after // Y, lax.rem(after, Y))
-    last_place = at(before // Y, lax.rem(before, Y))
     others = [peer(lax.rem(tp + i, SLOTS)) for i in range(1, SLOTS)]
 
+    barrier = pltpu.get_barrier_semaphore()
+    greeted = [*place.values(), *others]
+    for device in greeted:
+        pl.semaphore_signal(barrier, inc=1, device_id=device, device_id_type=MESH)
     mine = pl.ds(pl.multiple_of(fs * ROWS, ROWS), ROWS)
     for i in range(5):
         columns = slice(128 * i, 128 * i + 128)
@@ -155,10 +157,6 @@
     full1[mine, 384:] = w_out[...]
     act[tp] = stream[...]
 
-    barrier = pltpu.get_barrier_semaphore()
-    greeted = [*place.values(), *others, next_place, last_place]
-    for device in greeted:
-        pl.semaphore_signal(barrier, inc=1, device_id=device, device_id_type=MESH)
     pl.semaphore_wait(barrier, len(greeted))
 
     def remote(copy):

time: 138 us -> 138 us (level)
  no operation moved by 1% of the time
where the time goes in v5:
time: 138 us; the launch traced here: 137 us
  Pallas kernels  136 us (99%)
  local copies, waits for them, and re-layouts  1.57 us (1%)
    pallas_call x1, Pallas kernels, whole_layer(): pl.pallas_call(kernel, out_shape=jax.ShapeDtypeStruct(arrays[0].shape, BF...  136 us

profile of v5, /device:TPU:1, one launch (start us, length us, event | category | flops | bytes accessed | tf_op | source)
XLA Modules:
  0.0 137.5 jit_solution(13031678084035012015)
XLA Ops:
  0.0 135.9 %shard_map.100 = bf16[256,256]{1,0:T(8,128)(2,1)} custom-call(bf16[256,256]{1,0:T(8,128)(2,1)} %refs_0_.1, f32[6,2048]{1,0:T(8,128)} %refs_1_.1, bf16[64,704]{1,0:T(8,128)(2,1)} %refs_2_.1, bf16[64,704]{1,0:T(8,128)(2,1)} %refs_3_.1, bf16[64,704]{1,0:T(8,128)(2,1)} %bitcast.2, bf16[64,128]{1,0:T(8,128)(2,1)} %refs_5_.1, bf16[64,128]{1,0:T(8,128)(2,1)} %refs_6_.1, ...), custom_call_target="tpu_custom_call" | custom-call | tf_op jit(solution)/shard_map/pallas_call | solution.py:417
  135.9 1.6 %copy.12 = bf16[256,256]{1,0:T(8,128)(2,1)} copy(bf16[256,256]{1,0:T(8,128)(2,1)} %shard_map.100) | data formatting | bytes 262144
